TPU v7x, 256 devices: a 2x2x32 block of a 4x8x32 slice. The times are simulated.
256 devices in a mesh: grp: 4 (over y, x), ep: 32 (over z), tp: 2 (over core).
Axes of the slice: x: 2, y: 2, z: 32, core: 2. Of those that a mesh axis runs over, the one named last changes fastest.
The devices are a block of a 4x8x32 slice.
Arguments:
- tokens: bfloat16 [8192, 2048], P(('grp', 'ep')), parts along dimension 0, may hold values from -6 to 6
- norm_gain: float32 [2048], replicated, may hold values from 0.1 to 1.9
- groups: int32 [8192], P(('grp', 'ep')), parts along dimension 0, may hold values from 0 to 1, as said below
- picks: int32 [8192, 4], P(('grp', 'ep')), parts along dimension 0, may hold values from 0 to 31, as said below
- gates: float32 [8192, 4], P(('grp', 'ep')), parts along dimension 0, may hold values from 0.1 to 1
- w_gate: bfloat16 [64, 2048, 512], P('ep', None, 'tp'), may hold values from -0.125 to 0.125
- w_up: bfloat16 [64, 2048, 512], P('ep', None, 'tp'), may hold values from -0.125 to 0.125
- w_down: bfloat16 [64, 512, 2048], P('ep', 'tp'), may hold values from -0.25 to 0.25
Outputs:
- mixed: bfloat16 [8192, 2048], P(('grp', 'ep'), 'tp'), parts along dimension 0
There are 4 independent parts, one for each index of `grp`. A program takes and returns all parts, laid end to end along the dimension named above; an argument that names none is the same for every part. Nothing has to cross between parts.
Inputs may be any that keep to these rules, and one draw needn't show every extreme that they name: `groups`: among the tokens of one device, exactly 8 lie in one common group and all of them name one common expert of it as their first pick; every other token of that device lies in another group. A token's 4 picks are distinct. Among the tokens of one device at most 8 name any one expert (group and pick together), and in every draw one expert is named by exactly 8 tokens of every device.
All inputs are finite; a program needn't handle non-finite values.
Results may differ from a plain program's by a relative error of at most 0.014.
Values may be sent and summed in bfloat16 or wider, within the bound.
A program may use at most 64 MiB of HBM per device.

v0:
```python
import jax
import jax.numpy as jnp
from jax import lax
from jax.sharding import PartitionSpec as P

GROUPS = 2


epsilon = 1e-06


def in_blocks(x, dim, count):
    shape = x.shape
    pieces = x.reshape(*shape[:dim], count, shape[dim] // count, *shape[dim + 1 :])
    return jnp.moveaxis(pieces, dim, 0)


def summed_on_arrival(x, axis, dim):
    pieces = in_blocks(x, dim, lax.axis_size(axis))
    arrived = lax.all_to_all(pieces, axis, split_axis=0, concat_axis=0, tiled=True)
    return arrived.astype(jnp.float32).sum(axis=0)


def in_order(pieces, dim):
    shape = list(pieces.shape[1:])
    shape[dim] *= pieces.shape[0]
    return jnp.moveaxis(pieces, 0, dim).reshape(shape)


def copy_for_each(x, axis):
    copies = jnp.broadcast_to(x, (lax.axis_size(axis), *x.shape))
    return lax.all_to_all(copies, axis, split_axis=0, concat_axis=0, tiled=True)


def collect(x, axis, dim):
    return in_order(copy_for_each(x, axis), dim)


def run_expert(rows, w_gate, w_up, w_down):
    gate_pre = jnp.einsum("sjiw,jwf->sjif", rows, w_gate, preferred_element_type=jnp.float32)
    up_pre = jnp.einsum("sjiw,jwf->sjif", rows, w_up, preferred_element_type=jnp.float32)
    hidden = (jax.nn.silu(gate_pre) * up_pre).astype(jnp.bfloat16)
    partial_sum = jnp.einsum(
        "sjif,jfw->sjiw", hidden, w_down, preferred_element_type=jnp.float32
    ).astype(jnp.bfloat16)
    return summed_on_arrival(partial_sum, "tp", 3).astype(jnp.bfloat16)


def on_device(tokens, norm_gain, groups, picks, gates, w_gate, w_up, w_down):
    tok_rows, width = tokens.shape
    top = picks.shape[1]
    local = w_gate.shape[0]
    senders = lax.axis_size("ep")
    experts = senders * local
    group_experts = experts // GROUPS
    capacity = tok_rows * top // group_experts
    values = tokens.astype(jnp.float32)
    normed = (
        values * lax.rsqrt(jnp.mean(values * values, axis=-1, keepdims=True) + epsilon) * norm_gain
    ).astype(jnp.bfloat16)
    expert_id = groups[:, None] * group_experts + picks
    count = tok_rows * top
    flat_ids = expert_id.reshape(count)
    onehot = (flat_ids[:, None] == jnp.arange(experts, dtype=jnp.int32)[None, :]).astype(jnp.int32)
    before = jnp.cumsum(onehot, axis=0) - onehot
    target = flat_ids * capacity + jnp.sum(before * onehot, axis=1)
    place = (target[:, None] == jnp.arange(experts * capacity, dtype=jnp.int32)[None, :]).astype(
        jnp.float32
    )
    owner = (
        (jnp.arange(count, dtype=jnp.int32) // top)[:, None]
        == jnp.arange(tok_rows, dtype=jnp.int32)[None, :]
    ).astype(jnp.float32)
    spread = jnp.dot(place.T, owner, precision=lax.Precision.HIGHEST).astype(jnp.bfloat16)
    buffer = jnp.dot(spread, normed, preferred_element_type=jnp.float32).astype(jnp.bfloat16)
    buffer = buffer.reshape(senders, local, capacity, width)
    half = width // lax.axis_size("tp")
    buffer = lax.dynamic_slice_in_dim(buffer, lax.axis_index("tp") * half, half, 3)
    received = lax.all_to_all(buffer, "ep", split_axis=0, concat_axis=0, tiled=True)
    received = collect(received, "tp", 3)
    result = run_expert(received, w_gate, w_up, w_down)
    returned = lax.all_to_all(result, "ep", split_axis=0, concat_axis=0, tiled=True)
    weighted = place * gates.reshape(count)[:, None]
    combine = jnp.dot(owner.T, weighted, precision=lax.Precision.HIGHEST)
    flat_out = returned.reshape(experts * capacity, returned.shape[3]).astype(jnp.float32)
    mixed = jnp.dot(combine, flat_out, precision=lax.Precision.HIGHEST).astype(jnp.bfloat16)
    return mixed


def solution(mesh):
    in_specs = (
        P(("grp", "ep"), None),
        P(),
        P(("grp", "ep")),
        P(("grp", "ep"), None),
        P(("grp", "ep"), None),
        P("ep", None, "tp"),
        P("ep", None, "tp"),
        P("ep", "tp", None),
    )
    out_specs = P(("grp", "ep"), "tp")
    return jax.shard_map(
        on_device, mesh=mesh, in_specs=in_specs, out_specs=out_specs, check_vma=False
    )
```

profile of v0, /device:TPU:37, one launch (start us, length us, event | category | flops | bytes accessed | tf_op | source)
XLA Modules:
  0.0 283.0 jit_solution(16782573616001933310)
XLA Ops:
  0.0 0.0 copy-start
  0.0 0.8 broadcast_multiply_fusion
  0.8 0.7 broadcast_add_fusion
  1.5 0.1 copy.32
  1.6 0.1 eq.61
  1.7 0.1 reshape.65
  1.8 0.6 reduce-window.6
  2.4 0.2 slice_reduce_fusion
  2.7 0.1 fusion.39
  2.8 1.1 fusion.19
  3.9 0.3 convolution_convert_fusion.3
  4.2 1.7 convolution_convert_fusion.1
  5.9 0.1 constant_dynamic-slice_fusion
  6.1 137.5 %all_to_all.20 = bf16[32,2,8,1024]{3,2,1,0:T(8,128)(2,1)S(1)} all-to-all(bf16[32,2,8,1024]{3,2,1,0:T(8,128)(2,1)S(1)} %constant_dynamic-slice_fusion), channel_id=1, replica_groups=mesh['grp'=4,'ep'=32,'tp'=2] {'ep'}, dimensions={0} | all-to-all | bytes 2097152 | tf_op jit(solution)/shard_map/all_to_all | solution.py:79
  143.5 0.1 copy.36
  143.6 0.2 broadcast_in_dim.2
  143.9 5.9 %all_to_all.21 = bf16[2,32,2,8,1024]{4,3,1,2,0:T(8,128)(2,1)S(1)} all-to-all(bf16[2,32,2,8,1024]{4,3,1,2,0:T(8,128)(2,1)S(1)} %broadcast_in_dim.2), channel_id=1, replica_groups=mesh['grp'=4,'ep'=32,'tp'=2] {'tp'}, dimensions={0} | all-to-all | bytes 4194304 | tf_op jit(solution)/shard_map/all_to_all | solution.py:32
  149.8 0.0 copy-start.2
  149.8 0.2 copy.37
  150.0 0.0 copy-start.1
  150.1 1.3 copy-done.1
  151.4 0.8 copy-done.2
  152.1 0.7 fusion.5
  152.9 0.0 copy-done
  152.9 4.8 %convolution_convert_fusion = bf16[2,32,8,2048]{3,2,1,0:T(8,128)(2,1)} fusion(bf16[2,256,2048]{2,1,0:T(8,128)(2,1)S(1)} %copy-done, bf16[32,2,8,2048]{3,2,0,1:T(8,128)(2,1)} %bitcast.70, bf16[2,2048,256]{2,1,0:T(8,128)(2,1)} %param.14, f32[32,2,8,256]{3,2,0,1:T(8,128)S(1)} %fusion.5), kind=kOutput, calls=%fused_computation | convolution fusion | flops 1075576832 | bytes 8912896 | tf_op jit(solution)/shard_map/sjif,jfw->sjiw/dot_general | solution.py:43
  157.7 1.8 copy.48
  159.5 6.3 %all_to_all.22 = bf16[2,32,2,8,1024]{4,3,1,2,0:T(8,128)(2,1)} all-to-all(bf16[2,32,2,8,1024]{4,3,1,2,0:T(8,128)(2,1)S(1)} %bitcast.72), channel_id=1, replica_groups=mesh['grp'=4,'ep'=32,'tp'=2] {'tp'}, dimensions={0} | all-to-all | bytes 4194304 | tf_op jit(solution)/shard_map/all_to_all | solution.py:20
  165.8 2.2 reduce_sum.32
  168.0 0.0 copy-start.3
  168.1 1.1 copy.40
  169.1 7.9 %all-to-all-start.3 = ((bf16[32,2,8,1024]{3,2,1,0:T(8,128)(2,1)}), bf16[32,2,8,1024]{3,2,1,0:T(8,128)(2,1)S(1)}, u32[]{:S(2)}, u32[]{:S(2)}) async-start(bf16[32,2,8,1024]{3,2,1,0:T(8,128)(2,1)} %copy.40), calls=%async_computation.3 | async-start | bytes 2097152 | tf_op jit(solution)/shard_map/all_to_all | solution.py:82
  177.0 0.0 copy-done.3
  177.0 0.1 copy.35
  177.1 0.1 mul.64
  177.2 0.4 fusion.27
  177.6 104.0 %all-to-all-done.3 = bf16[32,2,8,1024]{3,2,1,0:T(8,128)(2,1)S(1)} async-done(((bf16[32,2,8,1024]{3,2,1,0:T(8,128)(2,1)}), bf16[32,2,8,1024]{3,2,1,0:T(8,128)(2,1)S(1)}, u32[]{:S(2)}, u32[]{:S(2)}) %all-to-all-start.3) | async-done | bytes 1048608 | tf_op jit(solution)/shard_map/all_to_all | solution.py:82
  281.7 1.3 convolution_convert_fusion.2
  (5 shorter events, 0.1 us)
Async XLA Ops:
  0.0 152.9 %copy-start = (bf16[2,256,2048]{2,1,0:T(8,128)(2,1)S(1)}, bf16[2,256,2048]{2,1,0:T(8,128)(2,1)}, u32[]{:S(2)}) copy-start(bf16[2,256,2048]{2,1,0:T(8,128)(2,1)} %param.15) | copy-start | bytes 6291460
  149.8 2.3 copy-start.2
  150.0 1.4 copy-start.1
  168.0 9.0 %copy-start.3 = (f32[64,4]{0,1:T(4,128)S(1)}, f32[64,4]{0,1:T(4,128)}, u32[]{:S(2)}) copy-start(f32[64,4]{0,1:T(4,128)} %param.12) | copy-start | bytes 3076
  169.1 112.5 %all-to-all-start.3 = ((bf16[32,2,8,1024]{3,2,1,0:T(8,128)(2,1)}), bf16[32,2,8,1024]{3,2,1,0:T(8,128)(2,1)S(1)}, u32[]{:S(2)}, u32[]{:S(2)}) async-start(bf16[32,2,8,1024]{3,2,1,0:T(8,128)(2,1)} %copy.40), calls=%async_computation.3 | async-start | bytes 2097152 | tf_op jit(solution)/shard_map/all_to_all | solution.py:82
where the time goes:
time: 283 us
  blocking collectives  150 us (53%)
  waiting for transfers between devices  104 us (37%)
  matrix products  9.31 us (3%)
  starting transfers between devices  7.85 us (3%)
  local copies, waits for them, and re-layouts  6.31 us (2%)
  other arithmetic  5.6 us (2%)
    all_to_all x1, blocking collectives, on_device(): lax.all_to_all(buffer, 'ep', split_axis=0, concat_axis=0, tiled=True)  137 us
    all_to_all x1, waiting for transfers between devices, on_device(): lax.all_to_all(result, 'ep', split_axis=0, concat_axis=0, tiled=True)  104 us
    all_to_all x1, starting transfers between devices, on_device(): lax.all_to_all(result, 'ep', split_axis=0, concat_axis=0, tiled=True)  7.85 us
    all_to_all x1, blocking collectives, summed_on_arrival(): lax.all_to_all(pieces, axis, split_axis=0, concat_axis=0, tiled=True)  6.33 us
    all_to_all x1, blocking collectives, copy_for_each(): return lax.all_to_all(copies, axis, split_axis=0, concat_axis=0, tiled=True)  5.94 us
  transfers between devices with their start and end apart: 1, of which 1 were waited for; matrix products, arithmetic and copies ran while one was open for 0% of the time, Pallas kernels for 0%

commit v1 on v0

v1 whole, which is shorter than its diff:
```python
import functools

import jax
import jax.numpy as jnp
from jax import lax
from jax.experimental import pallas as pl
from jax.experimental.pallas import tpu as pltpu
from jax.sharding import PartitionSpec as P

GROUPS = 2
MESH = pl.DeviceIdType.MESH
F32 = jnp.float32
BF16 = jnp.bfloat16
CW = 256
META = 16
BATCH = 4

epsilon = 1e-06


def dot(a, b):
    return jnp.dot(a, b, preferred_element_type=F32)


def kernel(
    n, rows, width, local, cap, ffl,
    tok_ref, gain_ref, meta_ref, wg_hbm, wu_hbm, wd_hbm, out_ref,
    own, ag, rs, rs0, contrib, wg, wu, wd, x_own, x_sib, p_own, p_sib, p_rcv, fin,
    sel, gsel, meta_s, rank_s, upper, hid,
    ag_ss, ag_rs, rs_ss, rs_rs, x_ss, x_rs, p_ss, p_rs, f_ss, f_rs, w_sem, own_sem,
):
    slots = n // 2
    batches = slots // BATCH
    nch = width // CW
    half_ch = nch // 2
    me = lax.axis_index("ep")
    tp = lax.axis_index("tp")
    right, left = lax.rem(me + 1, n), lax.rem(me + n - 1, n)
    ahead = jnp.where(tp == 1, right, left)
    behind = jnp.where(tp == 1, left, right)
    reach = slots - 1 + tp
    sibling = 1 - tp

    barrier = pltpu.get_barrier_semaphore()
    pl.semaphore_signal(barrier, inc=1, device_id={"ep": right}, device_id_type=MESH)
    pl.semaphore_signal(barrier, inc=1, device_id={"ep": left}, device_id_type=MESH)
    pl.semaphore_signal(barrier, inc=1, device_id={"tp": sibling}, device_id_type=MESH)

    w_copies = [
        pltpu.make_async_copy(src, dst, w_sem.at[i])
        for i, (src, dst) in enumerate(((wg_hbm, wg), (wu_hbm, wu), (wd_hbm, wd)))
    ]
    for copy in w_copies:
        copy.start()

    m = meta_ref[...]
    hi = m.astype(BF16).astype(F32)
    mid = (m - hi).astype(BF16).astype(F32)
    low = m - hi - mid
    row16 = lax.broadcasted_iota(jnp.int32, m.shape, 0)
    own[0:META, :] = jnp.where(row16 < 8, hi, jnp.where(row16 < 12, mid, low)).astype(BF16)

    total = jnp.zeros((rows, 1), F32)
    for c in range(nch):
        v = tok_ref[:, c * CW:(c + 1) * CW].astype(F32)
        total = total + jnp.sum(v * v, axis=1, keepdims=True)
    scale = lax.rsqrt(total / width + epsilon)
    for c in range(nch):
        v = tok_ref[:, c * CW:(c + 1) * CW].astype(F32)
        own[META + rows * c:META + rows * (c + 1), :] = (
            v * scale * gain_ref[:, c * CW:(c + 1) * CW]
        ).astype(BF16)

    ri = lax.broadcasted_iota(jnp.int32, (BATCH * rows, BATCH * rows), 0)
    ci = lax.broadcasted_iota(jnp.int32, (BATCH * rows, BATCH * rows), 1)
    upper[...] = jnp.where((ri // rows == ci // rows) & (ri < ci), 1.0, 0.0).astype(BF16)

    own_copy = pltpu.make_async_copy(own, ag.at[slots - 1], own_sem)

    @pl.when(tp == 0)
    def _():
        own_copy.start()

    pl.semaphore_wait(barrier, 3)

    def span(c):
        if c == 0:
            return pl.ds(0, META + rows)
        return pl.ds(META + rows * c, rows)

    def ag_copy(src, k, c):
        return pltpu.make_async_remote_copy(
            src_ref=src.at[span(c)],
            dst_ref=ag.at[k, span(c)],
            send_sem=ag_ss.at[k],
            recv_sem=ag_rs.at[k, c],
            device_id={"ep": ahead},
            device_id_type=MESH,
        )

    for c in range(nch):
        ag_copy(own, 0, c).start()

    for copy in w_copies:
        copy.wait()

    @pl.when(tp == 0)
    def _():
        own_copy.wait()

    def x_copy(b):
        return pltpu.make_async_remote_copy(
            src_ref=x_own.at[b], dst_ref=x_sib.at[b], send_sem=x_ss.at[b],
            recv_sem=x_rs.at[b], device_id={"tp": sibling}, device_id_type=MESH,
        )

    def p_copy(b):
        return pltpu.make_async_remote_copy(
            src_ref=p_sib.at[b], dst_ref=p_rcv.at[b], send_sem=p_ss.at[b],
            recv_sem=p_rs.at[b], device_id={"tp": sibling}, device_id_type=MESH,
        )

    wide = BATCH * rows
    each = BATCH * cap

    def ag_step(b, j, c):
        k = b * BATCH + j
        if j < BATCH - 2:
            ag_copy(own, k, c).wait_recv()
            ag_copy(ag.at[k], k + 1, c).start()
        elif j == BATCH - 2:
            ag_copy(own, k, c).wait_recv()

            @pl.when(k <= reach - 2)
            def _():
                ag_copy(ag.at[k], k + 1, c).start()
        else:
            @pl.when(k <= reach - 1)
            def _():
                ag_copy(own, k, c).wait_recv()

            @pl.when(k <= reach - 2)
            def _():
                ag_copy(ag.at[k], k + 1, c).start()

    def routing(b):
        lane = lax.broadcasted_iota(jnp.int32, (META, wide), 1) // rows
        mm = ag[b * BATCH, 0:META, :].astype(F32)
        for j in range(1, BATCH):
            mm = jnp.where(lane == j, ag[b * BATCH + j, 0:META, :].astype(F32), mm)
        meta_s[...] = mm
        ids = [meta_s[k:k + 1, :] for k in range(4)]
        parts = [[meta_s[4 * (p + 1) + k:4 * (p + 1) + k + 1, :] for k in range(4)] for p in range(3)]
        row8 = lax.broadcasted_iota(jnp.int32, (8, wide), 0)
        members, gates = [], []
        for e in range(local):
            eid = (me * local + e).astype(F32)
            hits = [jnp.where(i == eid, 1.0, 0.0) for i in ids]
            members.append(sum(hits))
            gates.append([sum(h * g for h, g in zip(hits, part)) for part in parts])
        stacked = jnp.zeros((8, wide), F32)
        for e in range(local):
            stacked = jnp.where(row8 == e, members[e], stacked)
        rank_s[...] = dot(stacked.astype(BF16), upper[...])
        block = lax.broadcasted_iota(jnp.int32, (1, wide), 1) // rows
        row = lax.broadcasted_iota(jnp.int32, (each, wide), 0)
        for e in range(local):
            rank = rank_s[e:e + 1, :].astype(jnp.int32)
            key = jnp.where(members[e] > 0.5, block * cap + rank, -1)
            pick = jnp.where(row == key, 1.0, 0.0)
            sel[e * each:(e + 1) * each, :] = pick.astype(BF16)
            for p in range(3):
                at = (p * local + e) * each
                gsel[at:at + each, :] = (pick * gates[e][p]).astype(BF16)

    def select(b, c):
        block = jnp.concatenate(
            [ag[b * BATCH + j, META + rows * c:META + rows * (c + 1), :] for j in range(BATCH)], axis=0
        )
        x_own[b, :, c * CW:(c + 1) * CW] = dot(sel[...], block).astype(BF16)

    def expert_in(b, e):
        return jnp.concatenate(
            [x_own[b, e * each:(e + 1) * each, :], x_sib[b, e * each:(e + 1) * each, :]], axis=0
        )

    def gate_up(b, e):
        x = expert_in(b, e)
        gate = dot(x, wg[e])
        up = dot(x, wu[e])
        hid[e] = (gate / (1.0 + jnp.exp(-gate)) * up).astype(BF16)

    def down(b, e, part):
        cols = slice(part * width // 2, (part + 1) * width // 2)
        y = dot(hid[e], wd[e, :, cols]).astype(BF16)
        p_own[b, e * each:(e + 1) * each, cols] = y[:each]
        p_sib[b, e * each:(e + 1) * each, cols] = y[each:]

    def combine(b, c):
        cols = slice(c * CW, (c + 1) * CW)
        y = (p_own[b, :, cols].astype(F32) + p_rcv[b, :, cols].astype(F32)).astype(BF16)
        stacked = jnp.concatenate([y, y, y], axis=0)
        g = lax.dot_general(
            gsel[...], stacked, (((0,), (0,)), ((), ())), preferred_element_type=F32
        )
        for j in range(BATCH):
            contrib[b * BATCH + j, :, cols] = g[j * rows:(j + 1) * rows]

    def pieces(b):
        def start_x():
            for c in range(nch // 2, nch):
                select(b, c)
            x_copy(b).start()

        def first_half():
            for c in range(nch // 2):
                select(b, c)

        def wait_x():
            x_copy(b).wait_recv()
            gate_up(b, 0)

        def last_down():
            down(b, local - 1, 1)
            p_copy(b).start()

        def wait_p():
            p_copy(b).wait_recv()
            for c in range(nch // 2):
                combine(b, c)

        def rest():
            for c in range(nch // 2, nch):
                combine(b, c)

        return {
            0: functools.partial(routing, b),
            1: first_half,
            2: start_x,
            5: wait_x,
            6: functools.partial(down, b, 0, 0),
            7: functools.partial(down, b, 0, 1),
            8: functools.partial(gate_up, b, 1),
            9: functools.partial(down, b, 1, 0),
            10: last_down,
            14: wait_p,
            15: rest,
        }

    def window(b, _):
        work = pieces(b - 1)
        steps = [(j, c) for j in range(BATCH) for c in range(nch)]
        per = len(steps) // 16
        for i in range(16):
            @pl.when(b < batches)
            def _():
                for j, c in steps[i * per:(i + 1) * per]:
                    ag_step(b, j, c)

            if i in work:
                pl.when(b > 0)(work[i])
        return 0

    lax.fori_loop(0, batches + 1, window, 0)

    def rs_copy(src, d, c):
        return pltpu.make_async_remote_copy(
            src_ref=src.at[c],
            dst_ref=rs.at[d, c],
            send_sem=rs_ss.at[d],
            recv_sem=rs_rs.at[d, c],
            device_id={"ep": behind},
            device_id_type=MESH,
        )

    for c in range(nch):
        rs0[c] = contrib[reach - 1, :, c * CW:(c + 1) * CW].astype(BF16)
        rs_copy(rs0, reach - 1, c).start()

    def rs_step(i, _):
        d = reach - 1 - i

        @pl.when(d >= 1)
        def _():
            for c in range(nch):
                rs_copy(rs0, d, c).wait_recv()
                rs[d, c] = (
                    rs[d, c].astype(F32) + contrib[d - 1, :, c * CW:(c + 1) * CW]
                ).astype(BF16)
                rs_copy(rs.at[d], d - 1, c).start()
        return 0

    lax.fori_loop(0, slots - 1, rs_step, 0)

    share = (1 - tp).astype(F32)

    def f_copy(c):
        return pltpu.make_async_remote_copy(
            src_ref=rs.at[0, sibling * half_ch + c], dst_ref=fin.at[c], send_sem=f_ss.at[c],
            recv_sem=f_rs.at[c], device_id={"tp": sibling}, device_id_type=MESH,
        )

    for c in range(nch):
        rs_copy(rs0, 0, c).wait_recv()
    for c in range(half_ch):
        at = sibling * half_ch + c
        cols = pl.ds(pl.multiple_of(at * CW, CW), CW)
        rs[0, at] = (rs[0, at].astype(F32) + share * contrib[slots - 1, :, cols]).astype(BF16)
        f_copy(c).start()
    for c in range(half_ch):
        at = tp * half_ch + c
        cols = pl.ds(pl.multiple_of(at * CW, CW), CW)
        f_copy(c).wait_recv()
        out_ref[:, c * CW:(c + 1) * CW] = (
            rs[0, at].astype(F32) + share * contrib[slots - 1, :, cols] + fin[c].astype(F32)
        ).astype(BF16)

    def drain(k, _):
        @pl.when(k <= reach - 1)
        def _():
            pltpu.make_async_remote_copy(
                src_ref=ag.at[k], dst_ref=ag.at[k], send_sem=ag_ss.at[k], recv_sem=ag_rs.at[k, 0],
                device_id={"ep": ahead}, device_id_type=MESH,
            ).wait_send()
            pltpu.make_async_remote_copy(
                src_ref=rs.at[k], dst_ref=rs.at[k], send_sem=rs_ss.at[k], recv_sem=rs_rs.at[k, 0],
                device_id={"ep": behind}, device_id_type=MESH,
            ).wait_send()
        return 0

    lax.fori_loop(0, slots, drain, 0)
    for b in range(batches):
        x_copy(b).wait_send()
        p_copy(b).wait_send()
    for c in range(half_ch):
        f_copy(c).wait_send()


def on_device(tokens, norm_gain, groups, picks, gates, w_gate, w_up, w_down):
    rows, width = tokens.shape
    top = picks.shape[1]
    local, _, ffl = w_gate.shape
    n = lax.axis_size("ep")
    group_experts = n * local // GROUPS
    cap = rows * top // group_experts
    slots = n // 2
    batches = slots // BATCH
    nch = width // CW
    ids = (groups[:, None] * group_experts + picks).astype(F32)
    meta = jnp.concatenate([ids.T, gates.T, gates.T, gates.T], axis=0)
    meta = jnp.tile(meta, (1, BATCH))
    batch_rows = local * BATCH * cap
    vmem = pltpu.VMEM
    dma = pltpu.SemaphoreType.DMA
    return pl.pallas_call(
        functools.partial(kernel, n, rows, width, local, cap, ffl),
        out_shape=jax.ShapeDtypeStruct((rows, width // 2), BF16),
        in_specs=[pl.BlockSpec(memory_space=pltpu.VMEM)] * 3 + [pl.BlockSpec(memory_space=pl.ANY)] * 3,
        out_specs=pl.BlockSpec(memory_space=pltpu.VMEM),
        scratch_shapes=[
            vmem((META + rows * nch, CW), BF16),
            vmem((slots, META + rows * nch, CW), BF16),
            vmem((slots, nch, rows, CW), BF16),
            vmem((nch, rows, CW), BF16),
            vmem((slots, rows, width), F32),
            vmem(w_gate.shape, BF16),
            vmem(w_up.shape, BF16),
            vmem(w_down.shape, BF16),
            vmem((batches, batch_rows, width), BF16),
            vmem((batches, batch_rows, width), BF16),
            vmem((batches, batch_rows, width), BF16),
            vmem((batches, batch_rows, width), BF16),
            vmem((batches, batch_rows, width), BF16),
            vmem((nch // 2, rows, CW), BF16),
            vmem((batch_rows, BATCH * rows), BF16),
            vmem((3 * batch_rows, BATCH * rows), BF16),
            vmem((META, BATCH * rows), F32),
            vmem((8, BATCH * rows), F32),
            vmem((BATCH * rows, BATCH * rows), BF16),
            vmem((local, 2 * BATCH * cap, ffl), BF16),
            dma((slots,)), dma((slots, nch)), dma((slots,)), dma((slots, nch)),
            dma((batches,)), dma((batches,)), dma((batches,)), dma((batches,)),
            dma((nch // 2,)), dma((nch // 2,)), dma((3,)), dma,
        ],
        compiler_params=pltpu.CompilerParams(
            collective_id=0, has_side_effects=True, vmem_limit_bytes=60 * 2**20
        ),
    )(tokens, norm_gain.reshape(1, width), meta, w_gate, w_up, w_down)


def solution(mesh):
    in_specs = (
        P(("grp", "ep"), None),
        P(),
        P(("grp", "ep")),
        P(("grp", "ep"), None),
        P(("grp", "ep"), None),
        P("ep", None, "tp"),
        P("ep", None, "tp"),
        P("ep", "tp", None),
    )
    out_specs = P(("grp", "ep"), "tp")
    return jax.shard_map(
        on_device, mesh=mesh, in_specs=in_specs, out_specs=out_specs, check_vma=False
    )
```

time: 283 us -> 139 us (0.49)
  blocking collectives: 150 us -> 0 us
  Pallas kernels: 0 us -> 135 us
  waiting for transfers between devices: 104 us -> 0 us
  matrix products: 9.31 us -> 0 us
  starting transfers between devices: 7.85 us -> 0 us
  local copies, waits for them, and re-layouts: 6.31 us -> 2.27 us
  other arithmetic: 5.6 us -> 2.14 us
    all_to_all x3 -> x0, blocking collectives: 150 us -> none  [the longest x1 137 us: on_device(): lax.all_to_all(buffer, 'ep', split_axis=0, concat_axis=0, tiled=True)]
    pallas_call x0 -> x1, Pallas kernels: none -> 135 us  [on_device(): pl.pallas_call(functools.partial(kernel, n, rows, width, local, cap, ffl)...]
    all_to_all x1 -> x0, waiting for transfers between devices: 104 us -> none  [on_device(): lax.all_to_all(result, 'ep', split_axis=0, concat_axis=0, tiled=True)]
    dot_general x6 -> x0, matrix products: 9.31 us -> none  [the longest x1 4.85 us: run_expert(): jnp.einsum('sjif,jfw->sjiw', hidden, w_down, preferred_element_type=jnp.f...]
    all_to_all x1 -> x0, starting transfers between devices: 7.85 us -> none  [on_device(): lax.all_to_all(result, 'ep', split_axis=0, concat_axis=0, tiled=True)]
    reduce_sum x3 -> x0, other arithmetic: 3.44 us -> none  [the longest x1 2.22 us: summed_on_arrival(): return arrived.astype(jnp.float32).sum(axis=0)]
  transfers between devices with their start and end apart: 1 -> 0, of which waited for: 1 -> 0; matrix products, arithmetic and copies ran while one was open for 0% -> 0% of each run, Pallas kernels for 0% -> 0%
where the time goes in v1:
time: 139 us
  Pallas kernels  135 us (97%)
  local copies, waits for them, and re-layouts  2.27 us (2%)
  other arithmetic  2.14 us (2%)
    pallas_call x1, Pallas kernels, on_device(): pl.pallas_call(functools.partial(kernel, n, rows, width, local, cap, ffl)...  135 us

profile of v1, /device:TPU:37, one launch (start us, length us, event | category | flops | bytes accessed | tf_op | source)
XLA Modules:
  0.0 139.1 jit_solution(13252779162490589262)
XLA Ops:
  0.0 0.7 broadcast_multiply_fusion
  0.7 0.7 convert_bitcast_fusion
  1.3 0.8 pad_maximum_fusion
  2.2 0.7 tile.10.meta_ref
  2.8 134.7 %shard_map.82 = bf16[64,1024]{1,0:T(8,128)(2,1)} custom-call(bf16[64,2048]{1,0:T(8,128)(2,1)} %tok_ref.1, f32[1,2048]{1,0:T(1,128)} %bitcast.4, f32[16,256]{1,0:T(8,128)} %tile.10.meta_ref, bf16[2,2048,256]{2,1,0:T(8,128)(2,1)} %wg_hbm.1, bf16[2,2048,256]{2,1,0:T(8,128)(2,1)} %wu_hbm.1, bf16[2,256,2048]{2,1,0:T(8,128)(2,1)} %wd_hbm.1), custom_call_target="tpu_custom_call" | custom-call | tf_op jit(solution)/shard_map/pallas_call | solution.py:355
  137.6 1.6 %copy.10 = bf16[64,1024]{1,0:T(8,128)(2,1)} copy(bf16[64,1024]{1,0:T(8,128)(2,1)} %shard_map.82) | data formatting | bytes 262144
  (1 shorter events, 0.0 us)

commit v2 on v1

v2 whole, which is shorter than its diff:
```python
import functools

import jax
import jax.numpy as jnp
from jax import lax
from jax.experimental import pallas as pl
from jax.experimental.pallas import tpu as pltpu
from jax.sharding import PartitionSpec as P

GROUPS = 2
MESH = pl.DeviceIdType.MESH
F32 = jnp.float32
BF16 = jnp.bfloat16
CW = 256
META = 16
BATCH = 4

epsilon = 1e-06


def dot(a, b):
    return jnp.dot(a, b, preferred_element_type=F32)


def tdot(a, b):
    return lax.dot_general(a, b, (((0,), (0,)), ((), ())), preferred_element_type=F32)


def kernel(
    n, rows, width, local, cap, group_experts,
    tok_ref, gain_ref, grp_ref, pick_ref, gate_ref, wg_hbm, wu_hbm, wd_hbm, out_ref,
    own, ag, rs, rs0, contrib, wg, wu, wd, x_own, x_sib, p_own, p_sib, p_rcv, fin,
    sel, gsel, meta_s, rank_s, upper, hid, perm,
    ag_ss, ag_rs, rs_ss, rs_rs, x_ss, x_rs, p_ss, p_rs, f_ss, f_rs, w_sem, own_sem,
):
    slots = n // 2
    batches = slots // BATCH
    last = batches - 1
    nch = width // CW
    half_ch = nch // 2
    me = lax.axis_index("ep")
    tp = lax.axis_index("tp")
    right, left = lax.rem(me + 1, n), lax.rem(me + n - 1, n)
    ahead = jnp.where(tp == 1, right, left)
    behind = jnp.where(tp == 1, left, right)
    reach = slots - 1 + tp
    sibling = 1 - tp

    barrier = pltpu.get_barrier_semaphore()
    pl.semaphore_signal(barrier, inc=1, device_id={"ep": right}, device_id_type=MESH)
    pl.semaphore_signal(barrier, inc=1, device_id={"ep": left}, device_id_type=MESH)
    pl.semaphore_signal(barrier, inc=1, device_id={"tp": sibling}, device_id_type=MESH)

    w_copies = [
        pltpu.make_async_copy(src, dst, w_sem.at[i])
        for i, (src, dst) in enumerate(((wg_hbm, wg), (wu_hbm, wu), (wd_hbm, wd)))
    ]
    for copy in w_copies:
        copy.start()

    def need(k):
        return min(rows, local * cap * (slots - k))

    ri = lax.broadcasted_iota(jnp.int32, (rows, rows), 0)
    ci = lax.broadcasted_iota(jnp.int32, (rows, rows), 1)
    group = jnp.sum(jnp.where(ri == ci, grp_ref[...].astype(F32), 0.0), axis=1, keepdims=True)
    ids = group * group_experts + pick_ref[...].astype(F32)
    chip = lax.div(ids.astype(jnp.int32), jnp.full(ids.shape, local, jnp.int32))
    dist = (chip - me) * (2 * tp - 1) + n
    dist = jnp.where(dist >= n, dist - n, dist)
    dist = jnp.where(dist <= reach, dist, 0).astype(F32)
    far = jnp.max(dist, axis=1, keepdims=True)
    far_row = jnp.sum(jnp.where(ri == ci, far, 0.0), axis=0, keepdims=True)
    before = (far_row > far) | ((far_row == far) & (ci < ri))
    place = jnp.sum(jnp.where(before, 1.0, 0.0), axis=1, keepdims=True).astype(jnp.int32)
    lane = lax.rem(
        lax.broadcasted_iota(jnp.int32, (rows, BATCH * rows), 1),
        jnp.full((rows, BATCH * rows), rows, jnp.int32),
    )
    perm[...] = jnp.where(lane == place, 1.0, 0.0).astype(BF16)

    g = gate_ref[...]
    hi = g.astype(BF16).astype(F32)
    mid = (g - hi).astype(BF16).astype(F32)
    low = g - hi - mid
    for i, part in enumerate((ids, hi, mid, low)):
        meta_s[4 * i:4 * (i + 1), :] = tdot(part.astype(BF16), perm[...])
    own[0:META, :] = meta_s[...].astype(BF16)

    total = jnp.zeros((rows, 1), F32)
    for c in range(nch):
        v = tok_ref[:, c * CW:(c + 1) * CW].astype(F32)
        total = total + jnp.sum(v * v, axis=1, keepdims=True)
    scale = lax.rsqrt(total / width + epsilon)
    for c in range(nch):
        v = tok_ref[:, c * CW:(c + 1) * CW].astype(F32)
        normed = (v * scale * gain_ref[:, c * CW:(c + 1) * CW]).astype(BF16)
        own[META + rows * c:META + rows * (c + 1), :] = tdot(perm[:, 0:rows], normed).astype(BF16)

    for k in range(slots):
        if need(k) < rows:
            for c in range(nch):
                ag[k, META + rows * c + need(k):META + rows * (c + 1), :] = jnp.zeros(
                    (rows - need(k), CW), BF16
                )

    bi = lax.broadcasted_iota(jnp.int32, (BATCH * rows, BATCH * rows), 0)
    bj = lax.broadcasted_iota(jnp.int32, (BATCH * rows, BATCH * rows), 1)
    upper[...] = jnp.where((bi // rows == bj // rows) & (bi < bj), 1.0, 0.0).astype(BF16)

    own_copy = pltpu.make_async_copy(own, ag.at[0], own_sem)

    pl.semaphore_wait(barrier, 3)

    def span(c, count):
        if c == 0:
            return pl.ds(0, META + count)
        return pl.ds(META + rows * c, count)

    def ag_copy(src, k, c, count=rows):
        return pltpu.make_async_remote_copy(
            src_ref=src.at[span(c, count)],
            dst_ref=ag.at[k, span(c, count)],
            send_sem=ag_ss.at[k],
            recv_sem=ag_rs.at[k, c],
            device_id={"ep": ahead},
            device_id_type=MESH,
        )

    for c in range(nch):
        ag_copy(own, 1 - tp, c).start()

    @pl.when(tp == 0)
    def _():
        own_copy.start()
        own_copy.wait()

    half_cols = width // 2

    def x_copy(b, h):
        return pltpu.make_async_remote_copy(
            src_ref=x_own.at[b, h], dst_ref=x_sib.at[b, h], send_sem=x_ss.at[b, h],
            recv_sem=x_rs.at[b, h], device_id={"tp": sibling}, device_id_type=MESH,
        )

    def p_copy(b, h):
        return pltpu.make_async_remote_copy(
            src_ref=p_sib.at[b, h], dst_ref=p_rcv.at[b, h], send_sem=p_ss.at[b, h],
            recv_sem=p_rs.at[b, h], device_id={"tp": sibling}, device_id_type=MESH,
        )

    wide = BATCH * rows
    each = BATCH * cap

    def routing(b):
        lane = lax.broadcasted_iota(jnp.int32, (META, wide), 1) // rows
        mm = ag[b * BATCH, 0:META, :].astype(F32)
        for j in range(1, BATCH):
            mm = jnp.where(lane == j, ag[b * BATCH + j, 0:META, :].astype(F32), mm)
        meta_s[...] = mm
        ids = [meta_s[k:k + 1, :] for k in range(4)]
        parts = [[meta_s[4 * (p + 1) + k:4 * (p + 1) + k + 1, :] for k in range(4)] for p in range(3)]
        row8 = lax.broadcasted_iota(jnp.int32, (8, wide), 0)
        members, gates = [], []
        for e in range(local):
            eid = (me * local + e).astype(F32)
            hits = [jnp.where(i == eid, 1.0, 0.0) for i in ids]
            members.append(sum(hits))
            gates.append([sum(h * g for h, g in zip(hits, part)) for part in parts])
        stacked = jnp.zeros((8, wide), F32)
        for e in range(local):
            stacked = jnp.where(row8 == e, members[e], stacked)
        rank_s[...] = dot(stacked.astype(BF16), upper[...])
        block = lax.broadcasted_iota(jnp.int32, (1, wide), 1) // rows
        row = lax.broadcasted_iota(jnp.int32, (each, wide), 0)
        for e in range(local):
            rank = rank_s[e:e + 1, :].astype(jnp.int32)
            key = jnp.where(members[e] > 0.5, block * cap + rank, -1)
            pick = jnp.where(row == key, 1.0, 0.0)
            sel[e * each:(e + 1) * each, :] = pick.astype(BF16)
            for p in range(3):
                at = (p * local + e) * each
                gsel[at:at + each, :] = (pick * gates[e][p]).astype(BF16)

    def select(b, c):
        block = jnp.concatenate(
            [ag[b * BATCH + j, META + rows * c:META + rows * (c + 1), :] for j in range(BATCH)], axis=0
        )
        h, at = divmod(c, half_ch)
        x_own[b, h, :, at * CW:(at + 1) * CW] = dot(sel[...], block).astype(BF16)

    def expert_in(b, e, h):
        return jnp.concatenate(
            [x_own[b, h, e * each:(e + 1) * each, :], x_sib[b, h, e * each:(e + 1) * each, :]], axis=0
        )

    def gate_up(b, e):
        gate, up = 0.0, 0.0
        for h in range(2):
            x = expert_in(b, e, h)
            gate += dot(x, wg[e, h * half_cols:(h + 1) * half_cols, :])
            up += dot(x, wu[e, h * half_cols:(h + 1) * half_cols, :])
        hid[e] = (gate / (1.0 + jnp.exp(-gate)) * up).astype(BF16)

    def down(b, e, h):
        y = dot(hid[e], wd[e, :, h * half_cols:(h + 1) * half_cols]).astype(BF16)
        p_own[b, h, e * each:(e + 1) * each, :] = y[:each]
        p_sib[b, h, e * each:(e + 1) * each, :] = y[each:]

    def combine(b, c):
        h, at = divmod(c, half_ch)
        cols = slice(at * CW, (at + 1) * CW)
        y = (p_own[b, h, :, cols].astype(F32) + p_rcv[b, h, :, cols].astype(F32)).astype(BF16)
        g = tdot(gsel[...], jnp.concatenate([y, y, y], axis=0))
        for j in range(BATCH):
            contrib[b * BATCH + j, c] = g[j * rows:(j + 1) * rows]

    def run_all(*calls):
        def go():
            for call in calls:
                call()
        return go

    def pieces(b):
        call = functools.partial
        return {
            0: call(routing, b),
            1: run_all(*[call(select, b, c) for c in range(half_ch)], lambda: x_copy(b, 0).start()),
            2: run_all(*[call(select, b, c) for c in range(half_ch, nch)], lambda: x_copy(b, 1).start()),
            5: run_all(lambda: x_copy(b, 0).wait_recv(), lambda: x_copy(b, 1).wait_recv(), call(gate_up, b, 0)),
            6: call(down, b, 0, 0),
            7: call(down, b, 0, 1),
            8: call(gate_up, b, 1),
            9: run_all(call(down, b, 1, 0), lambda: p_copy(b, 0).start()),
            10: run_all(call(down, b, 1, 1), lambda: p_copy(b, 1).start()),
            14: run_all(lambda: p_copy(b, 0).wait_recv(), *[call(combine, b, c) for c in range(half_ch)]),
            15: run_all(lambda: p_copy(b, 1).wait_recv(), *[call(combine, b, c) for c in range(half_ch, nch)]),
        }

    def ag_step(b, j, c, final):
        k = b * BATCH + j
        if final:
            k = last * BATCH + j
            ag_copy(own, k, c, need(k)).wait_recv()
            if k < slots - 1:
                ag_copy(ag.at[k], k + 1, c, need(k + 1)).start()
        elif j == 0:
            @pl.when(k + tp >= 1)
            def _():
                ag_copy(own, k, c).wait_recv()
                ag_copy(ag.at[k], k + 1, c).start()
        else:
            ag_copy(own, k, c).wait_recv()
            ag_copy(ag.at[k], k + 1, c).start()

    order = [(j, c) for j in range(BATCH) for c in range(nch)]
    per = len(order) // 16

    def window(b, _):
        work = pieces(b - 1)
        for i in range(16):
            for j, c in order[i * per:(i + 1) * per]:
                ag_step(b, j, c, False)
            if i in work:
                pl.when(b > 0)(work[i])
            if i == 4:
                @pl.when(b == 1)
                def _():
                    for copy in w_copies:
                        copy.wait()
        return 0

    lax.fori_loop(0, last, window, 0)

    work = pieces(last - 1)
    for i in range(16):
        for j, c in order[i * per:(i + 1) * per]:
            if j == BATCH - 1:
                continue
            ag_step(last, j, c, True)
        if i in work and i < 14:
            work[i]()
    work[14]()
    work[15]()

    for c in range(nch):
        ag_step(last, BATCH - 1, c, True)
        if c == 0:
            routing(last)
        select(last, c)
        if c in (half_ch - 1, nch - 1):
            x_copy(last, c // half_ch).start()
    partial = {}
    for h in range(2):
        x_copy(last, h).wait_recv()
        for e in range(local):
            x = expert_in(last, e, h)
            for i, w in enumerate((wg, wu)):
                y = dot(x, w[e, h * half_cols:(h + 1) * half_cols, :])
                partial[e, i] = y if h == 0 else partial[e, i] + y
    for e in range(local):
        gate, up = partial[e, 0], partial[e, 1]
        hid[e] = (gate / (1.0 + jnp.exp(-gate)) * up).astype(BF16)
    for h in range(2):
        for e in range(local):
            down(last, e, h)
        p_copy(last, h).start()

    def rs_copy(src, k, at, count=rows):
        return pltpu.make_async_remote_copy(
            src_ref=src.at[at, pl.ds(0, count)],
            dst_ref=rs.at[k, at, pl.ds(0, count)],
            send_sem=rs_ss.at[k],
            recv_sem=rs_rs.at[k, at],
            device_id={"ep": behind},
            device_id_type=MESH,
        )

    def turn(c):
        at = c + sibling * half_ch
        return jnp.where(at >= nch, at - nch, at)

    for h in range(2):
        p_copy(last, h).wait_recv()
        for c in range(h * half_ch, (h + 1) * half_ch):
            combine(last, c)
            count = need(slots - 1)
            rs0[c] = contrib[slots - 1, c].astype(BF16)
            rs_copy(rs0, slots - 2, c, count).start()

    def rs_step(k, got, count):
        for c in range(nch):
            at = turn(c)
            rs_copy(rs0, k, at, got).wait_recv()
            rs[k, at, 0:got, :] = (
                rs[k, at, 0:got, :].astype(F32) + contrib[k, at, 0:got, :]
            ).astype(BF16)
            if got < count:
                rs[k, at, got:count, :] = contrib[k, at, got:count, :].astype(BF16)
            rs_copy(rs.at[k], k - 1, at, count).start()

    k = slots - 2
    while need(k + 1) < rows:
        rs_step(k, need(k + 1), need(k))
        k -= 1
    top_k = k

    def rs_loop(i, _):
        rs_step(top_k - i, rows, rows)
        return 0

    lax.fori_loop(0, top_k, rs_loop, 0)

    @pl.when(tp == 1)
    def _():
        for c in range(nch):
            at = turn(c)
            rs_copy(rs0, 0, at).wait_recv()
            rs[0, at] = (rs[0, at].astype(F32) + contrib[0, at]).astype(BF16)
            rs_copy(rs.at[0], slots, at).start()
    end = jnp.where(tp == 1, slots, 0)
    share = (1 - tp).astype(F32)

    def f_copy(c):
        return pltpu.make_async_remote_copy(
            src_ref=rs0.at[c], dst_ref=fin.at[c], send_sem=f_ss.at[c],
            recv_sem=f_rs.at[c], device_id={"tp": sibling}, device_id_type=MESH,
        )

    rs0_sent = pltpu.make_async_remote_copy(
        src_ref=rs0.at[:, pl.ds(0, need(slots - 1))], dst_ref=rs0.at[:, pl.ds(0, need(slots - 1))],
        send_sem=rs_ss.at[slots - 2], recv_sem=rs_rs.at[slots - 2, 0],
        device_id={"ep": behind}, device_id_type=MESH,
    )
    rs0_sent.wait_send()
    for c in range(nch):
        at = turn(c)
        rs_copy(rs0, end, at).wait_recv()
        v = (rs[end, at].astype(F32) + share * contrib[0, at]).astype(BF16)
        y = dot(perm[:, 0:rows], v)
        if c < half_ch:
            rs0[c] = y.astype(BF16)
            f_copy(c).start()
        else:
            i = c - half_ch
            f_copy(i).wait_recv()
            out_ref[:, i * CW:(i + 1) * CW] = (y + fin[i].astype(F32)).astype(BF16)

    def ag_sent(k, count):
        size = pl.ds(0, META + nch * count)
        pltpu.make_async_remote_copy(
            src_ref=ag.at[k, size], dst_ref=ag.at[k, size], send_sem=ag_ss.at[k],
            recv_sem=ag_rs.at[k, 0], device_id={"ep": ahead}, device_id_type=MESH,
        ).wait_send()

    def rs_sent(k, count):
        size = pl.ds(0, count)
        pltpu.make_async_remote_copy(
            src_ref=rs.at[k, :, size], dst_ref=rs.at[k, :, size], send_sem=rs_ss.at[k],
            recv_sem=rs_rs.at[k, 0], device_id={"ep": behind}, device_id_type=MESH,
        ).wait_send()

    @pl.when(tp == 1)
    def _():
        ag_sent(0, rows)
        rs_sent(slots, rows)

    for k in range(1, slots):
        ag_sent(k, need(k))
    for k in range(slots - 2):
        rs_sent(k, need(k + 1))
    for b in range(batches):
        for h in range(2):
            x_copy(b, h).wait_send()
            p_copy(b, h).wait_send()
    for c in range(half_ch):
        f_copy(c).wait_send()


def on_device(tokens, norm_gain, groups, picks, gates, w_gate, w_up, w_down):
    rows, width = tokens.shape
    top = picks.shape[1]
    local, _, ffl = w_gate.shape
    n = lax.axis_size("ep")
    group_experts = n * local // GROUPS
    cap = rows * top // group_experts
    slots = n // 2
    batches = slots // BATCH
    nch = width // CW
    batch_rows = local * BATCH * cap
    vmem = pltpu.VMEM
    dma = pltpu.SemaphoreType.DMA
    return pl.pallas_call(
        functools.partial(kernel, n, rows, width, local, cap, group_experts),
        out_shape=jax.ShapeDtypeStruct((rows, width // 2), BF16),
        in_specs=[pl.BlockSpec(memory_space=pltpu.VMEM)] * 5 + [pl.BlockSpec(memory_space=pl.ANY)] * 3,
        out_specs=pl.BlockSpec(memory_space=pltpu.VMEM),
        scratch_shapes=[
            vmem((META + rows * nch, CW), BF16),
            vmem((slots, META + rows * nch, CW), BF16),
            vmem((slots + 1, nch, rows, CW), BF16),
            vmem((nch, rows, CW), BF16),
            vmem((slots, nch, rows, CW), F32),
            vmem(w_gate.shape, BF16),
            vmem(w_up.shape, BF16),
            vmem(w_down.shape, BF16),
            vmem((batches, 2, batch_rows, width // 2), BF16),
            vmem((batches, 2, batch_rows, width // 2), BF16),
            vmem((batches, 2, batch_rows, width // 2), BF16),
            vmem((batches, 2, batch_rows, width // 2), BF16),
            vmem((batches, 2, batch_rows, width // 2), BF16),
            vmem((nch // 2, rows, CW), BF16),
            vmem((batch_rows, BATCH * rows), BF16),
            vmem((3 * batch_rows, BATCH * rows), BF16),
            vmem((META, BATCH * rows), F32),
            vmem((8, BATCH * rows), F32),
            vmem((BATCH * rows, BATCH * rows), BF16),
            vmem((local, 2 * BATCH * cap, ffl), BF16),
            vmem((rows, BATCH * rows), BF16),
            dma((slots,)), dma((slots, nch)), dma((slots + 1,)), dma((slots + 1, nch)),
            dma((batches, 2)), dma((batches, 2)), dma((batches, 2)), dma((batches, 2)),
            dma((nch // 2,)), dma((nch // 2,)), dma((3,)), dma,
        ],
        compiler_params=pltpu.CompilerParams(
            collective_id=0, has_side_effects=True, vmem_limit_bytes=60 * 2**20
        ),
    )(
        tokens, norm_gain.reshape(1, width), groups.reshape(1, rows), picks, gates,
        w_gate, w_up, w_down,
    )


def solution(mesh):
    in_specs = (
        P(("grp", "ep"), None),
        P(),
        P(("grp", "ep")),
        P(("grp", "ep"), None),
        P(("grp", "ep"), None),
        P("ep", None, "tp"),
        P("ep", None, "tp"),
        P("ep", "tp", None),
    )
    out_specs = P(("grp", "ep"), "tp")
    return jax.shard_map(
        on_device, mesh=mesh, in_specs=in_specs, out_specs=out_specs, check_vma=False
    )
```

time: 139 us -> 135 us (0.971)
  Pallas kernels: 135 us -> 130 us
  other arithmetic: 2.14 us -> 0 us
  local copies, waits for them, and re-layouts: 2.27 us -> 4.32 us
    pallas_call x1, Pallas kernels: 135 us -> 130 us  [on_device(): pl.pallas_call(functools.partial(kernel, n, rows, width, local, cap, grou...]
    unnamed x1 -> x3, local copies, waits for them, and re-layouts: 1.57 us -> 4.32 us
where the time goes in v2:
time: 135 us
  Pallas kernels  130 us (96%)
  local copies, waits for them, and re-layouts  4.32 us (3%)
    pallas_call x1, Pallas kernels, on_device(): pl.pallas_call(functools.partial(kernel, n, rows, width, local, cap, grou...  130 us
    unnamed x3, local copies, waits for them, and re-layouts  4.32 us

profile of v2, /device:TPU:37, one launch (start us, length us, event | category | flops | bytes accessed | tf_op | source)
XLA Modules:
  0.0 134.7 jit_solution(13167204120924674015)
XLA Ops:
  0.0 1.4 %copy.9.pick_ref = s32[64,4]{1,0:T(8,128)} copy(s32[64,4]{0,1:T(4,128)} %param.11) | data formatting | bytes 2048 | tf_op args[3]
  1.4 1.4 %copy.10.gate_ref = f32[64,4]{1,0:T(8,128)} copy(f32[64,4]{0,1:T(4,128)} %param.12) | data formatting | bytes 2048 | tf_op args[4]
  2.8 130.3 %shard_map.82 = bf16[64,1024]{1,0:T(8,128)(2,1)} custom-call(bf16[64,2048]{1,0:T(8,128)(2,1)} %tok_ref.1, f32[1,2048]{1,0:T(1,128)} %bitcast.2, s32[1,64]{1,0:T(1,128)} %bitcast.3, s32[64,4]{1,0:T(8,128)} %copy.9.pick_ref, f32[64,4]{1,0:T(8,128)} %copy.10.gate_ref, bf16[2,2048,256]{2,1,0:T(8,128)(2,1)} %wg_hbm.1, bf16[2,2048,256]{2,1,0:T(8,128)(2,1)} %wu_hbm.1, ...), custom_call_target="tpu_custom_call" | custom-call | tf_op jit(solution)/shard_map/pallas_call | solution.py:433
  133.1 1.6 %copy.12 = bf16[64,1024]{1,0:T(8,128)(2,1)} copy(bf16[64,1024]{1,0:T(8,128)(2,1)} %shard_map.82) | data formatting | bytes 262144

commit v3 on v2

--- a/solution.py
+++ b/solution.py
@@ -31,7 +31,7 @@
     tok_ref, gain_ref, grp_ref, pick_ref, gate_ref, wg_hbm, wu_hbm, wd_hbm, out_ref,
     own, ag, rs, rs0, contrib, wg, wu, wd, x_own, x_sib, p_own, p_sib, p_rcv, fin,
     sel, gsel, meta_s, rank_s, upper, hid, perm,
-    ag_ss, ag_rs, rs_ss, rs_rs, x_ss, x_rs, p_ss, p_rs, f_ss, f_rs, w_sem, own_sem,
+    ag_ss, got, rs_ss, x_ss, x_rs, p_ss, p_rs, f_ss, f_rs, w_sem, own_sem,
 ):
     slots = n // 2
     batches = slots // BATCH
@@ -58,19 +58,23 @@
     for copy in w_copies:
         copy.start()
 
+    split = rows // 2
+
+    def parts(count):
+        return [(lo, min(count, lo + split)) for lo in range(0, count, split)]
+
     def need(k):
         return min(rows, local * cap * (slots - k))
 
     ri = lax.broadcasted_iota(jnp.int32, (rows, rows), 0)
     ci = lax.broadcasted_iota(jnp.int32, (rows, rows), 1)
-    group = jnp.sum(jnp.where(ri == ci, grp_ref[...].astype(F32), 0.0), axis=1, keepdims=True)
-    ids = group * group_experts + pick_ref[...].astype(F32)
-    chip = lax.div(ids.astype(jnp.int32), jnp.full(ids.shape, local, jnp.int32))
+    ids = grp_ref[...] * group_experts + pick_ref[...]
+    chip = lax.div(ids, jnp.full(ids.shape, local, jnp.int32))
     dist = (chip - me) * (2 * tp - 1) + n
     dist = jnp.where(dist >= n, dist - n, dist)
     dist = jnp.where(dist <= reach, dist, 0).astype(F32)
-    far = jnp.max(dist, axis=1, keepdims=True)
-    far_row = jnp.sum(jnp.where(ri == ci, far, 0.0), axis=0, keepdims=True)
+    far_row = jnp.max(dist, axis=0, keepdims=True)
+    far = jnp.sum(jnp.where(ri == ci, far_row, 0.0), axis=1, keepdims=True)
     before = (far_row > far) | ((far_row == far) & (ci < ri))
     place = jnp.sum(jnp.where(before, 1.0, 0.0), axis=1, keepdims=True).astype(jnp.int32)
     lane = lax.rem(
@@ -83,19 +87,42 @@
     hi = g.astype(BF16).astype(F32)
     mid = (g - hi).astype(BF16).astype(F32)
     low = g - hi - mid
-    for i, part in enumerate((ids, hi, mid, low)):
-        meta_s[4 * i:4 * (i + 1), :] = tdot(part.astype(BF16), perm[...])
+    for i, part in enumerate((ids.astype(F32), hi, mid, low)):
+        meta_s[4 * i:4 * (i + 1), :] = dot(part.astype(BF16), perm[...])
     own[0:META, :] = meta_s[...].astype(BF16)
 
-    total = jnp.zeros((rows, 1), F32)
+    total = jnp.zeros((rows, CW), F32)
     for c in range(nch):
         v = tok_ref[:, c * CW:(c + 1) * CW].astype(F32)
-        total = total + jnp.sum(v * v, axis=1, keepdims=True)
-    scale = lax.rsqrt(total / width + epsilon)
+        total = total + v * v
+    scale = lax.rsqrt(jnp.sum(total, axis=1, keepdims=True) / width + epsilon)
+
+    def ag_copy(src, k, c, part):
+        lo, hi = part
+        first = 0 if c == 0 and lo == 0 else META + rows * c + lo
+        span = pl.ds(first, META + rows * c + hi - first)
+        return pltpu.make_async_remote_copy(
+            src_ref=src.at[span],
+            dst_ref=ag.at[k, span],
+            send_sem=ag_ss.at[k],
+            recv_sem=got.at[k, c, lo // split],
+            device_id={"ep": ahead},
+            device_id_type=MESH,
+        )
+
+    pl.semaphore_wait(barrier, 3)
     for c in range(nch):
         v = tok_ref[:, c * CW:(c + 1) * CW].astype(F32)
         normed = (v * scale * gain_ref[:, c * CW:(c + 1) * CW]).astype(BF16)
         own[META + rows * c:META + rows * (c + 1), :] = tdot(perm[:, 0:rows], normed).astype(BF16)
+        for part in parts(rows):
+            ag_copy(own, 1 - tp, c, part).start()
+
+    own_copy = pltpu.make_async_copy(own, ag.at[0], own_sem)
+
+    @pl.when(tp == 0)
+    def _():
+        own_copy.start()
 
     for k in range(slots):
         if need(k) < rows:
@@ -108,31 +135,8 @@
     bj = lax.broadcasted_iota(jnp.int32, (BATCH * rows, BATCH * rows), 1)
     upper[...] = jnp.where((bi // rows == bj // rows) & (bi < bj), 1.0, 0.0).astype(BF16)
 
-    own_copy = pltpu.make_async_copy(own, ag.at[0], own_sem)
-
-    pl.semaphore_wait(barrier, 3)
-
-    def span(c, count):
-        if c == 0:
-            return pl.ds(0, META + count)
-        return pl.ds(META + rows * c, count)
-
-    def ag_copy(src, k, c, count=rows):
-        return pltpu.make_async_remote_copy(
-            src_ref=src.at[span(c, count)],
-            dst_ref=ag.at[k, span(c, count)],
-            send_sem=ag_ss.at[k],
-            recv_sem=ag_rs.at[k, c],
-            device_id={"ep": ahead},
-            device_id_type=MESH,
-        )
-
-    for c in range(nch):
-        ag_copy(own, 1 - tp, c).start()
-
     @pl.when(tp == 0)
     def _():
-        own_copy.start()
         own_copy.wait()
 
     half_cols = width // 2
@@ -239,19 +243,21 @@
 
     def ag_step(b, j, c, final):
         k = b * BATCH + j
+
+        def both(k, count, ahead_count):
+            for part in parts(count):
+                ag_copy(own, k, c, part).wait_recv()
+                if part[0] < ahead_count:
+                    part = (part[0], min(part[1], ahead_count))
+                    ag_copy(ag.at[k], k + 1, c, part).start()
+
         if final:
             k = last * BATCH + j
-            ag_copy(own, k, c, need(k)).wait_recv()
-            if k < slots - 1:
-                ag_copy(ag.at[k], k + 1, c, need(k + 1)).start()
+            both(k, need(k), need(k + 1) if k < slots - 1 else 0)
         elif j == 0:
-            @pl.when(k + tp >= 1)
-            def _():
-                ag_copy(own, k, c).wait_recv()
-                ag_copy(ag.at[k], k + 1, c).start()
+            pl.when(k + tp >= 1)(lambda: both(k, rows, rows))
         else:
-            ag_copy(own, k, c).wait_recv()
-            ag_copy(ag.at[k], k + 1, c).start()
+            both(k, rows, rows)
 
     order = [(j, c) for j in range(BATCH) for c in range(nch)]
     per = len(order) // 16
@@ -306,12 +312,13 @@
             down(last, e, h)
         p_copy(last, h).start()
 
-    def rs_copy(src, k, at, count=rows):
+    def rs_copy(src, k, at, part):
+        span = pl.ds(part[0], part[1] - part[0])
         return pltpu.make_async_remote_copy(
-            src_ref=src.at[at, pl.ds(0, count)],
-            dst_ref=rs.at[k, at, pl.ds(0, count)],
+            src_ref=src.at[at, span],
+            dst_ref=rs.at[k, at, span],
             send_sem=rs_ss.at[k],
-            recv_sem=rs_rs.at[k, at],
+            recv_sem=got.at[k, at, part[0] // split],
             device_id={"ep": behind},
             device_id_type=MESH,
         )
@@ -326,18 +333,24 @@
             combine(last, c)
             count = need(slots - 1)
             rs0[c] = contrib[slots - 1, c].astype(BF16)
-            rs_copy(rs0, slots - 2, c, count).start()
-
-    def rs_step(k, got, count):
+            for part in parts(count):
+                rs_copy(rs0, slots - 2, c, part).start()
+
+    def rs_add(k, to, at, there, count):
+        for lo, hi in parts(count):
+            mid = max(lo, min(hi, there))
+            if lo < mid:
+                rs_copy(rs0, k, at, (lo, mid)).wait_recv()
+                rs[k, at, lo:mid, :] = (
+                    rs[k, at, lo:mid, :].astype(F32) + contrib[k, at, lo:mid, :]
+                ).astype(BF16)
+            if mid < hi:
+                rs[k, at, mid:hi, :] = contrib[k, at, mid:hi, :].astype(BF16)
+            rs_copy(rs.at[k], to, at, (lo, hi)).start()
+
+    def rs_step(k, there, count):
         for c in range(nch):
-            at = turn(c)
-            rs_copy(rs0, k, at, got).wait_recv()
-            rs[k, at, 0:got, :] = (
-                rs[k, at, 0:got, :].astype(F32) + contrib[k, at, 0:got, :]
-            ).astype(BF16)
-            if got < count:
-                rs[k, at, got:count, :] = contrib[k, at, got:count, :].astype(BF16)
-            rs_copy(rs.at[k], k - 1, at, count).start()
+            rs_add(k, k - 1, turn(c), there, count)
 
     k = slots - 2
     while need(k + 1) < rows:
@@ -354,10 +367,31 @@
     @pl.when(tp == 1)
     def _():
         for c in range(nch):
-            at = turn(c)
-            rs_copy(rs0, 0, at).wait_recv()
-            rs[0, at] = (rs[0, at].astype(F32) + contrib[0, at]).astype(BF16)
-            rs_copy(rs.at[0], slots, at).start()
+            rs_add(0, slots, turn(c), rows, rows)
+    def ag_sent(k, count):
+        size = pl.ds(0, META + nch * count)
+        pltpu.make_async_remote_copy(
+            src_ref=ag.at[k, size], dst_ref=ag.at[k, size], send_sem=ag_ss.at[k],
+            recv_sem=got.at[k, 0, 0], device_id={"ep": ahead}, device_id_type=MESH,
+        ).wait_send()
+
+    def rs_sent(k, count):
+        size = pl.ds(0, count)
+        pltpu.make_async_remote_copy(
+            src_ref=rs.at[k, :, size], dst_ref=rs.at[k, :, size], send_sem=rs_ss.at[k],
+            recv_sem=got.at[k, 0, 0], device_id={"ep": behind}, device_id_type=MESH,
+        ).wait_send()
+
+    pl.when(tp == 1)(functools.partial(ag_sent, 0, rows))
+    for k in range(1, slots):
+        ag_sent(k, need(k))
+    for b in range(batches):
+        for h in range(2):
+            x_copy(b, h).wait_send()
+            p_copy(b, h).wait_send()
+    for k in range(3, slots - 2):
+        rs_sent(k, need(k + 1))
+
     end = jnp.where(tp == 1, slots, 0)
     share = (1 - tp).astype(F32)
 
@@ -369,13 +403,14 @@
 
     rs0_sent = pltpu.make_async_remote_copy(
         src_ref=rs0.at[:, pl.ds(0, need(slots - 1))], dst_ref=rs0.at[:, pl.ds(0, need(slots - 1))],
-        send_sem=rs_ss.at[slots - 2], recv_sem=rs_rs.at[slots - 2, 0],
+        send_sem=rs_ss.at[slots - 2], recv_sem=got.at[slots - 2, 0, 0],
         device_id={"ep": behind}, device_id_type=MESH,
     )
     rs0_sent.wait_send()
     for c in range(nch):
         at = turn(c)
-        rs_copy(rs0, end, at).wait_recv()
+        for part in parts(rows):
+            rs_copy(rs0, end, at, part).wait_recv()
         v = (rs[end, at].astype(F32) + share * contrib[0, at]).astype(BF16)
         y = dot(perm[:, 0:rows], v)
         if c < half_ch:
@@ -386,33 +421,13 @@
             f_copy(i).wait_recv()
             out_ref[:, i * CW:(i + 1) * CW] = (y + fin[i].astype(F32)).astype(BF16)
 
-    def ag_sent(k, count):
-        size = pl.ds(0, META + nch * count)
-        pltpu.make_async_remote_copy(
-            src_ref=ag.at[k, size], dst_ref=ag.at[k, size], send_sem=ag_ss.at[k],
-            recv_sem=ag_rs.at[k, 0], device_id={"ep": ahead}, device_id_type=MESH,
-        ).wait_send()
-
-    def rs_sent(k, count):
-        size = pl.ds(0, count)
-        pltpu.make_async_remote_copy(
-            src_ref=rs.at[k, :, size], dst_ref=rs.at[k, :, size], send_sem=rs_ss.at[k],
-            recv_sem=rs_rs.at[k, 0], device_id={"ep": behind}, device_id_type=MESH,
-        ).wait_send()
+    for k in range(3):
+        rs_sent(k, need(k + 1))
 
     @pl.when(tp == 1)
     def _():
-        ag_sent(0, rows)
         rs_sent(slots, rows)
 
-    for k in range(1, slots):
-        ag_sent(k, need(k))
-    for k in range(slots - 2):
-        rs_sent(k, need(k + 1))
-    for b in range(batches):
-        for h in range(2):
-            x_copy(b, h).wait_send()
-            p_copy(b, h).wait_send()
     for c in range(half_ch):
         f_copy(c).wait_send()
 
@@ -432,7 +447,7 @@
     dma = pltpu.SemaphoreType.DMA
     return pl.pallas_call(
         functools.partial(kernel, n, rows, width, local, cap, group_experts),
-        out_shape=jax.ShapeDtypeStruct((rows, width // 2), BF16),
+        out_shape=pltpu.VMEM((rows, width // 2), BF16),
         in_specs=[pl.BlockSpec(memory_space=pltpu.VMEM)] * 5 + [pl.BlockSpec(memory_space=pl.ANY)] * 3,
         out_specs=pl.BlockSpec(memory_space=pltpu.VMEM),
         scratch_shapes=[
@@ -457,7 +472,7 @@
             vmem((BATCH * rows, BATCH * rows), BF16),
             vmem((local, 2 * BATCH * cap, ffl), BF16),
             vmem((rows, BATCH * rows), BF16),
-            dma((slots,)), dma((slots, nch)), dma((slots + 1,)), dma((slots + 1, nch)),
+            dma((slots,)), dma((slots + 1, nch, 2)), dma((slots + 1,)),
             dma((batches, 2)), dma((batches, 2)), dma((batches, 2)), dma((batches, 2)),
             dma((nch // 2,)), dma((nch // 2,)), dma((3,)), dma,
         ],
@@ -465,7 +480,7 @@
             collective_id=0, has_side_effects=True, vmem_limit_bytes=60 * 2**20
         ),
     )(
-        tokens, norm_gain.reshape(1, width), groups.reshape(1, rows), picks, gates,
+        tokens, norm_gain.reshape(1, width), groups.reshape(1, rows), picks.T, gates.T,
         w_gate, w_up, w_down,
     )
 

time: 135 us -> 128 us (0.948)
  local copies, waits for them, and re-layouts: 4.32 us -> 0.66 us
  Pallas kernels: 130 us -> 127 us
    unnamed x3 -> x1, local copies, waits for them, and re-layouts: 4.32 us -> 0.66 us
    pallas_call x1, Pallas kernels: 130 us -> 127 us  [on_device(): pl.pallas_call(functools.partial(kernel, n, rows, width, local, cap, grou...]
where the time goes in v3:
time: 128 us; the launch traced here: 127 us
  Pallas kernels  127 us (99%)
    pallas_call x1, Pallas kernels, on_device(): pl.pallas_call(functools.partial(kernel, n, rows, width, local, cap, grou...  127 us

profile of v3, /device:TPU:37, one launch (start us, length us, event | category | flops | bytes accessed | tf_op | source)
XLA Modules:
  0.0 127.4 jit_solution(11872772346837154014)
XLA Ops:
  0.0 126.8 %shard_map.82 = bf16[64,1024]{1,0:T(8,128)(2,1)S(1)} custom-call(bf16[64,2048]{1,0:T(8,128)(2,1)} %tok_ref.1, f32[1,2048]{1,0:T(1,128)} %bitcast.4, s32[1,64]{1,0:T(1,128)} %bitcast.7, s32[4,64]{1,0:T(4,128)} %bitcast.5, f32[4,64]{1,0:T(4,128)} %bitcast.6, bf16[2,2048,256]{2,1,0:T(8,128)(2,1)} %wg_hbm.1, bf16[2,2048,256]{2,1,0:T(8,128)(2,1)} %wu_hbm.1, ...), custom_call_target="tpu_custom_call" | custom-call | tf_op jit(solution)/shard_map/pallas_call | solution.py:448
  126.8 0.7 copy.10

commit v4 on v3

--- a/solution.py
+++ b/solution.py
@@ -12,6 +12,7 @@
 F32 = jnp.float32
 BF16 = jnp.bfloat16
 CW = 256
+LANES = 128
 META = 16
 BATCH = 4
 
@@ -30,7 +31,7 @@
     n, rows, width, local, cap, group_experts,
     tok_ref, gain_ref, grp_ref, pick_ref, gate_ref, wg_hbm, wu_hbm, wd_hbm, out_ref,
     own, ag, rs, rs0, contrib, wg, wu, wd, x_own, x_sib, p_own, p_sib, p_rcv, fin,
-    sel, gsel, meta_s, rank_s, upper, hid, perm,
+    sel, gsel, meta_s, rank_s, upper, hid, perm, skip,
     ag_ss, got, rs_ss, x_ss, x_rs, p_ss, p_rs, f_ss, f_rs, w_sem, own_sem,
 ):
     slots = n // 2
@@ -38,17 +39,20 @@
     last = batches - 1
     nch = width // CW
     half_ch = nch // 2
+    fine = width // LANES
     me = lax.axis_index("ep")
     tp = lax.axis_index("tp")
     right, left = lax.rem(me + 1, n), lax.rem(me + n - 1, n)
     ahead = jnp.where(tp == 1, right, left)
     behind = jnp.where(tp == 1, left, right)
+    ahead2 = lax.rem(ahead + ahead - me + n, n)
+    behind2 = lax.rem(behind + behind - me + n, n)
     reach = slots - 1 + tp
     sibling = 1 - tp
 
     barrier = pltpu.get_barrier_semaphore()
-    pl.semaphore_signal(barrier, inc=1, device_id={"ep": right}, device_id_type=MESH)
-    pl.semaphore_signal(barrier, inc=1, device_id={"ep": left}, device_id_type=MESH)
+    for peer in (ahead2, behind2, ahead, behind):
+        pl.semaphore_signal(barrier, inc=1, device_id={"ep": peer}, device_id_type=MESH)
     pl.semaphore_signal(barrier, inc=1, device_id={"tp": sibling}, device_id_type=MESH)
 
     w_copies = [
@@ -88,8 +92,8 @@
     mid = (g - hi).astype(BF16).astype(F32)
     low = g - hi - mid
     for i, part in enumerate((ids.astype(F32), hi, mid, low)):
-        meta_s[4 * i:4 * (i + 1), :] = dot(part.astype(BF16), perm[...])
-    own[0:META, :] = meta_s[...].astype(BF16)
+        meta_s[4 * i:4 * (i + 1), 0:LANES] = dot(part.astype(BF16), perm[:, 0:LANES])
+    own[0:META, :] = meta_s[:, 0:LANES].astype(BF16)
 
     total = jnp.zeros((rows, CW), F32)
     for c in range(nch):
@@ -97,26 +101,27 @@
         total = total + v * v
     scale = lax.rsqrt(jnp.sum(total, axis=1, keepdims=True) / width + epsilon)
 
-    def ag_copy(src, k, c, part):
-        lo, hi = part
-        first = 0 if c == 0 and lo == 0 else META + rows * c + lo
-        span = pl.ds(first, META + rows * c + hi - first)
+    def ag_copy(src, k, c, count, to=ahead):
+        first = 0 if c == 0 else META + rows * c
+        span = pl.ds(first, META + rows * c + count - first)
         return pltpu.make_async_remote_copy(
             src_ref=src.at[span],
             dst_ref=ag.at[k, span],
             send_sem=ag_ss.at[k],
-            recv_sem=got.at[k, c, lo // split],
-            device_id={"ep": ahead},
+            recv_sem=got.at[k, c],
+            device_id={"ep": to},
             device_id_type=MESH,
         )
 
-    pl.semaphore_wait(barrier, 3)
+    pl.semaphore_wait(barrier, 5)
     for c in range(nch):
         v = tok_ref[:, c * CW:(c + 1) * CW].astype(F32)
         normed = (v * scale * gain_ref[:, c * CW:(c + 1) * CW]).astype(BF16)
-        own[META + rows * c:META + rows * (c + 1), :] = tdot(perm[:, 0:rows], normed).astype(BF16)
-        for part in parts(rows):
-            ag_copy(own, 1 - tp, c, part).start()
+        sorted_rows = tdot(perm[:, 0:rows], normed).astype(BF16)
+        for i in range(CW // LANES):
+            at = c * (CW // LANES) + i
+            own[META + rows * at:META + rows * (at + 1), :] = sorted_rows[:, i * LANES:(i + 1) * LANES]
+            ag_copy(own, 1 - tp, at, rows).start()
 
     own_copy = pltpu.make_async_copy(own, ag.at[0], own_sem)
 
@@ -126,9 +131,9 @@
 
     for k in range(slots):
         if need(k) < rows:
-            for c in range(nch):
+            for c in range(fine):
                 ag[k, META + rows * c + need(k):META + rows * (c + 1), :] = jnp.zeros(
-                    (rows - need(k), CW), BF16
+                    (rows - need(k), LANES), BF16
                 )
 
     bi = lax.broadcasted_iota(jnp.int32, (BATCH * rows, BATCH * rows), 0)
@@ -157,11 +162,13 @@
     each = BATCH * cap
 
     def routing(b):
-        lane = lax.broadcasted_iota(jnp.int32, (META, wide), 1) // rows
-        mm = ag[b * BATCH, 0:META, :].astype(F32)
-        for j in range(1, BATCH):
-            mm = jnp.where(lane == j, ag[b * BATCH + j, 0:META, :].astype(F32), mm)
-        meta_s[...] = mm
+        per_tile = LANES // rows
+        lane = lax.broadcasted_iota(jnp.int32, (META, LANES), 1) // rows
+        for i in range(wide // LANES):
+            mm = ag[b * BATCH + i * per_tile, 0:META, :].astype(F32)
+            for j in range(1, per_tile):
+                mm = jnp.where(lane == j, ag[b * BATCH + i * per_tile + j, 0:META, :].astype(F32), mm)
+            meta_s[:, i * LANES:(i + 1) * LANES] = mm
         ids = [meta_s[k:k + 1, :] for k in range(4)]
         parts = [[meta_s[4 * (p + 1) + k:4 * (p + 1) + k + 1, :] for k in range(4)] for p in range(3)]
         row8 = lax.broadcasted_iota(jnp.int32, (8, wide), 0)
@@ -187,9 +194,13 @@
                 gsel[at:at + each, :] = (pick * gates[e][p]).astype(BF16)
 
     def select(b, c):
-        block = jnp.concatenate(
-            [ag[b * BATCH + j, META + rows * c:META + rows * (c + 1), :] for j in range(BATCH)], axis=0
-        )
+        block = jnp.concatenate([
+            jnp.concatenate(
+                [ag[b * BATCH + j, META + rows * at:META + rows * (at + 1), :] for j in range(BATCH)],
+                axis=0,
+            )
+            for at in range(c * (CW // LANES), (c + 1) * (CW // LANES))
+        ], axis=1)
         h, at = divmod(c, half_ch)
         x_own[b, h, :, at * CW:(at + 1) * CW] = dot(sel[...], block).astype(BF16)
 
@@ -245,21 +256,24 @@
         k = b * BATCH + j
 
         def both(k, count, ahead_count):
-            for part in parts(count):
-                ag_copy(own, k, c, part).wait_recv()
-                if part[0] < ahead_count:
-                    part = (part[0], min(part[1], ahead_count))
-                    ag_copy(ag.at[k], k + 1, c, part).start()
+            ag_copy(own, k, c, count).wait_recv()
+            ag_copy(ag.at[k], k + 1, c, ahead_count).start()
 
         if final:
             k = last * BATCH + j
-            both(k, need(k), need(k + 1) if k < slots - 1 else 0)
+            if k < slots - 2:
+                ag_copy(own, k, c, need(k)).wait_recv()
+                if k == slots - 3:
+                    ag_copy(ag.at[k], k + 2, c, need(k + 2), ahead2).start()
+                ag_copy(ag.at[k], k + 1, c, need(k + 1)).start()
+            else:
+                ag_copy(own, k, c, need(k)).wait_recv()
         elif j == 0:
             pl.when(k + tp >= 1)(lambda: both(k, rows, rows))
         else:
             both(k, rows, rows)
 
-    order = [(j, c) for j in range(BATCH) for c in range(nch)]
+    order = [(j, c) for j in range(BATCH) for c in range(fine)]
     per = len(order) // 16
 
     def window(b, _):
@@ -289,13 +303,15 @@
     work[14]()
     work[15]()
 
-    for c in range(nch):
+    for c in range(fine):
         ag_step(last, BATCH - 1, c, True)
         if c == 0:
             routing(last)
-        select(last, c)
-        if c in (half_ch - 1, nch - 1):
-            x_copy(last, c // half_ch).start()
+        done, odd = divmod(c + 1, CW // LANES)
+        if odd == 0:
+            select(last, done - 1)
+            if done in (half_ch, nch):
+                x_copy(last, done // half_ch - 1).start()
     partial = {}
     for h in range(2):
         x_copy(last, h).wait_recv()
@@ -318,8 +334,19 @@
             src_ref=src.at[at, span],
             dst_ref=rs.at[k, at, span],
             send_sem=rs_ss.at[k],
-            recv_sem=got.at[k, at, part[0] // split],
+            recv_sem=got.at[k, at * 2 + part[0] // split],
             device_id={"ep": behind},
+            device_id_type=MESH,
+        )
+
+    def skip_copy(c):
+        span = pl.ds(0, need(slots - 1))
+        return pltpu.make_async_remote_copy(
+            src_ref=rs0.at[c, span],
+            dst_ref=skip.at[c],
+            send_sem=rs_ss.at[slots - 1],
+            recv_sem=got.at[slots + 1, c],
+            device_id={"ep": behind2},
             device_id_type=MESH,
         )
 
@@ -331,16 +358,21 @@
         p_copy(last, h).wait_recv()
         for c in range(h * half_ch, (h + 1) * half_ch):
             combine(last, c)
-            count = need(slots - 1)
-            rs0[c] = contrib[slots - 1, c].astype(BF16)
+            rs0[c, 0:need(slots - 1), :] = contrib[slots - 1, c, 0:need(slots - 1), :].astype(BF16)
+            skip_copy(c).start()
+            k, count = slots - 2, need(slots - 2)
+            rs[k, c, 0:count, :] = contrib[k, c, 0:count, :].astype(BF16)
             for part in parts(count):
-                rs_copy(rs0, slots - 2, c, part).start()
-
-    def rs_add(k, to, at, there, count):
+                rs_copy(rs.at[k], k - 1, c, part).start()
+
+    def rs_add(k, to, at, there, count, skipped=0):
         for lo, hi in parts(count):
             mid = max(lo, min(hi, there))
             if lo < mid:
                 rs_copy(rs0, k, at, (lo, mid)).wait_recv()
+                if lo < skipped:
+                    skip_copy(at).wait_recv()
+                    contrib[k, at, lo:skipped, :] += skip[at].astype(F32)
                 rs[k, at, lo:mid, :] = (
                     rs[k, at, lo:mid, :].astype(F32) + contrib[k, at, lo:mid, :]
                 ).astype(BF16)
@@ -348,11 +380,13 @@
                 rs[k, at, mid:hi, :] = contrib[k, at, mid:hi, :].astype(BF16)
             rs_copy(rs.at[k], to, at, (lo, hi)).start()
 
-    def rs_step(k, there, count):
+    def rs_step(k, there, count, skipped=0):
         for c in range(nch):
-            rs_add(k, k - 1, turn(c), there, count)
-
-    k = slots - 2
+            rs_add(k, k - 1, turn(c), there, count, skipped)
+
+    k = slots - 3
+    rs_step(k, need(k + 1), need(k), need(slots - 1))
+    k -= 1
     while need(k + 1) < rows:
         rs_step(k, need(k + 1), need(k))
         k -= 1
@@ -369,17 +403,17 @@
         for c in range(nch):
             rs_add(0, slots, turn(c), rows, rows)
     def ag_sent(k, count):
-        size = pl.ds(0, META + nch * count)
+        size = pl.ds(0, META + fine * count)
         pltpu.make_async_remote_copy(
             src_ref=ag.at[k, size], dst_ref=ag.at[k, size], send_sem=ag_ss.at[k],
-            recv_sem=got.at[k, 0, 0], device_id={"ep": ahead}, device_id_type=MESH,
+            recv_sem=got.at[k, 0], device_id={"ep": ahead}, device_id_type=MESH,
         ).wait_send()
 
     def rs_sent(k, count):
         size = pl.ds(0, count)
         pltpu.make_async_remote_copy(
             src_ref=rs.at[k, :, size], dst_ref=rs.at[k, :, size], send_sem=rs_ss.at[k],
-            recv_sem=got.at[k, 0, 0], device_id={"ep": behind}, device_id_type=MESH,
+            recv_sem=got.at[k, 0], device_id={"ep": behind}, device_id_type=MESH,
         ).wait_send()
 
     pl.when(tp == 1)(functools.partial(ag_sent, 0, rows))
@@ -401,12 +435,11 @@
             recv_sem=f_rs.at[c], device_id={"tp": sibling}, device_id_type=MESH,
         )
 
-    rs0_sent = pltpu.make_async_remote_copy(
-        src_ref=rs0.at[:, pl.ds(0, need(slots - 1))], dst_ref=rs0.at[:, pl.ds(0, need(slots - 1))],
-        send_sem=rs_ss.at[slots - 2], recv_sem=got.at[slots - 2, 0, 0],
-        device_id={"ep": behind}, device_id_type=MESH,
-    )
-    rs0_sent.wait_send()
+    size = pl.ds(0, need(slots - 1))
+    pltpu.make_async_remote_copy(
+        src_ref=rs0.at[:, size], dst_ref=rs0.at[:, size], send_sem=rs_ss.at[slots - 1],
+        recv_sem=got.at[slots - 1, 0], device_id={"ep": behind2}, device_id_type=MESH,
+    ).wait_send()
     for c in range(nch):
         at = turn(c)
         for part in parts(rows):
@@ -451,8 +484,8 @@
         in_specs=[pl.BlockSpec(memory_space=pltpu.VMEM)] * 5 + [pl.BlockSpec(memory_space=pl.ANY)] * 3,
         out_specs=pl.BlockSpec(memory_space=pltpu.VMEM),
         scratch_shapes=[
-            vmem((META + rows * nch, CW), BF16),
-            vmem((slots, META + rows * nch, CW), BF16),
+            vmem((META + rows * width // LANES, LANES), BF16),
+            vmem((slots, META + rows * width // LANES, LANES), BF16),
             vmem((slots + 1, nch, rows, CW), BF16),
             vmem((nch, rows, CW), BF16),
             vmem((slots, nch, rows, CW), F32),
@@ -472,7 +505,8 @@
             vmem((BATCH * rows, BATCH * rows), BF16),
             vmem((local, 2 * BATCH * cap, ffl), BF16),
             vmem((rows, BATCH * rows), BF16),
-            dma((slots,)), dma((slots + 1, nch, 2)), dma((slots + 1,)),
+            vmem((nch, local * cap, CW), BF16),
+            dma((slots,)), dma((slots + 2, width // LANES)), dma((slots + 1,)),
             dma((batches, 2)), dma((batches, 2)), dma((batches, 2)), dma((batches, 2)),
             dma((nch // 2,)), dma((nch // 2,)), dma((3,)), dma,
         ],

time: 128 us -> 125 us (0.977)
  Pallas kernels: 127 us -> 124 us
    pallas_call x1, Pallas kernels: 127 us -> 124 us  [on_device(): pl.pallas_call(functools.partial(kernel, n, rows, width, local, cap, grou...]
where the time goes in v4:
time: 125 us
  Pallas kernels  124 us (99%)
    pallas_call x1, Pallas kernels, on_device(): pl.pallas_call(functools.partial(kernel, n, rows, width, local, cap, grou...  124 us

profile of v4, /device:TPU:37, one launch (start us, length us, event | category | flops | bytes accessed | tf_op | source)
XLA Modules:
  0.0 125.1 jit_solution(16343101504337627086)
XLA Ops:
  0.0 124.5 %shard_map.82 = bf16[64,1024]{1,0:T(8,128)(2,1)S(1)} custom-call(bf16[64,2048]{1,0:T(8,128)(2,1)} %tok_ref.1, f32[1,2048]{1,0:T(1,128)} %bitcast.4, s32[1,64]{1,0:T(1,128)} %bitcast.7, s32[4,64]{1,0:T(4,128)} %bitcast.5, f32[4,64]{1,0:T(4,128)} %bitcast.6, bf16[2,2048,256]{2,1,0:T(8,128)(2,1)} %wg_hbm.1, bf16[2,2048,256]{2,1,0:T(8,128)(2,1)} %wu_hbm.1, ...), custom_call_target="tpu_custom_call" | custom-call | tf_op jit(solution)/shard_map/pallas_call | solution.py:481
  124.5 0.7 copy.10

commit v5 on v4

--- a/solution.py
+++ b/solution.py
@@ -31,7 +31,7 @@
     n, rows, width, local, cap, group_experts,
     tok_ref, gain_ref, grp_ref, pick_ref, gate_ref, wg_hbm, wu_hbm, wd_hbm, out_ref,
     own, ag, rs, rs0, contrib, wg, wu, wd, x_own, x_sib, p_own, p_sib, p_rcv, fin,
-    sel, gsel, meta_s, rank_s, upper, hid, perm, skip,
+    sel, gsel, meta_s, rank_s, upper, hid, perm, skip, acc,
     ag_ss, got, rs_ss, x_ss, x_rs, p_ss, p_rs, f_ss, f_rs, w_sem, own_sem,
 ):
     slots = n // 2
@@ -209,48 +209,55 @@
             [x_own[b, h, e * each:(e + 1) * each, :], x_sib[b, h, e * each:(e + 1) * each, :]], axis=0
         )
 
-    def gate_up(b, e):
-        gate, up = 0.0, 0.0
-        for h in range(2):
-            x = expert_in(b, e, h)
-            gate += dot(x, wg[e, h * half_cols:(h + 1) * half_cols, :])
-            up += dot(x, wu[e, h * half_cols:(h + 1) * half_cols, :])
+    def half(h):
+        return pl.ds(pl.multiple_of(h * half_cols, half_cols), half_cols)
+
+    def activate(e, gate, up):
         hid[e] = (gate / (1.0 + jnp.exp(-gate)) * up).astype(BF16)
+
+    def gate_up(b, e, h):
+        x = expert_in(b, e, h)
+        gate = dot(x, wg[e, h * half_cols:(h + 1) * half_cols, :])
+        up = dot(x, wu[e, h * half_cols:(h + 1) * half_cols, :])
+        if h == 0:
+            acc[0], acc[1] = gate, up
+        else:
+            activate(e, acc[0] + gate, acc[1] + up)
 
     def down(b, e, h):
         y = dot(hid[e], wd[e, :, h * half_cols:(h + 1) * half_cols]).astype(BF16)
         p_own[b, h, e * each:(e + 1) * each, :] = y[:each]
         p_sib[b, h, e * each:(e + 1) * each, :] = y[each:]
 
-    def combine(b, c):
-        h, at = divmod(c, half_ch)
+    def combine(b, h, at):
         cols = slice(at * CW, (at + 1) * CW)
         y = (p_own[b, h, :, cols].astype(F32) + p_rcv[b, h, :, cols].astype(F32)).astype(BF16)
         g = tdot(gsel[...], jnp.concatenate([y, y, y], axis=0))
         for j in range(BATCH):
-            contrib[b * BATCH + j, c] = g[j * rows:(j + 1) * rows]
-
-    def run_all(*calls):
-        def go():
-            for call in calls:
-                call()
-        return go
+            contrib[b * BATCH + j, h * half_ch + at] = g[j * rows:(j + 1) * rows]
 
     def pieces(b):
         call = functools.partial
-        return {
-            0: call(routing, b),
-            1: run_all(*[call(select, b, c) for c in range(half_ch)], lambda: x_copy(b, 0).start()),
-            2: run_all(*[call(select, b, c) for c in range(half_ch, nch)], lambda: x_copy(b, 1).start()),
-            5: run_all(lambda: x_copy(b, 0).wait_recv(), lambda: x_copy(b, 1).wait_recv(), call(gate_up, b, 0)),
-            6: call(down, b, 0, 0),
-            7: call(down, b, 0, 1),
-            8: call(gate_up, b, 1),
-            9: run_all(call(down, b, 1, 0), lambda: p_copy(b, 0).start()),
-            10: run_all(call(down, b, 1, 1), lambda: p_copy(b, 1).start()),
-            14: run_all(lambda: p_copy(b, 0).wait_recv(), *[call(combine, b, c) for c in range(half_ch)]),
-            15: run_all(lambda: p_copy(b, 1).wait_recv(), *[call(combine, b, c) for c in range(half_ch, nch)]),
-        }
+        work = {0: [call(routing, b)]}
+        for c in range(nch):
+            work[1 + c] = [call(select, b, c)]
+        for h in range(2):
+            work[(h + 1) * half_ch].append(lambda h=h: x_copy(b, h).start())
+            work[12 + h] = [lambda h=h: x_copy(b, h).wait_recv(), call(gate_up, b, 0, h)]
+            work[14 + h] = [call(down, b, 0, h)]
+            work[16 + h] = [call(gate_up, b, 1, h)]
+            work[18 + h] = [call(down, b, 1, h), lambda h=h: p_copy(b, h).start()]
+            for at in range(half_ch):
+                work[24 + h * half_ch + at] = [call(combine, b, h, at)]
+            work[24 + h * half_ch].insert(0, lambda h=h: p_copy(b, h).wait_recv())
+
+        def joined(calls):
+            def go():
+                for each_call in calls:
+                    each_call()
+            return go
+
+        return {at: joined(calls) for at, calls in work.items()}
 
     def ag_step(b, j, c, final):
         k = b * BATCH + j
@@ -274,16 +281,17 @@
             both(k, rows, rows)
 
     order = [(j, c) for j in range(BATCH) for c in range(fine)]
-    per = len(order) // 16
+    places = 32
+    per = len(order) // places
 
     def window(b, _):
         work = pieces(b - 1)
-        for i in range(16):
+        for i in range(places):
             for j, c in order[i * per:(i + 1) * per]:
                 ag_step(b, j, c, False)
             if i in work:
                 pl.when(b > 0)(work[i])
-            if i == 4:
+            if i == 10:
                 @pl.when(b == 1)
                 def _():
                     for copy in w_copies:
@@ -293,15 +301,12 @@
     lax.fori_loop(0, last, window, 0)
 
     work = pieces(last - 1)
-    for i in range(16):
-        for j, c in order[i * per:(i + 1) * per]:
-            if j == BATCH - 1:
-                continue
+    lead = [(j, c) for j, c in order if j < BATCH - 1]
+    for i in range(places):
+        for j, c in lead[i * len(lead) // places:(i + 1) * len(lead) // places]:
             ag_step(last, j, c, True)
-        if i in work and i < 14:
+        if i in work:
             work[i]()
-    work[14]()
-    work[15]()
 
     for c in range(fine):
         ag_step(last, BATCH - 1, c, True)
@@ -321,12 +326,15 @@
                 y = dot(x, w[e, h * half_cols:(h + 1) * half_cols, :])
                 partial[e, i] = y if h == 0 else partial[e, i] + y
     for e in range(local):
-        gate, up = partial[e, 0], partial[e, 1]
-        hid[e] = (gate / (1.0 + jnp.exp(-gate)) * up).astype(BF16)
-    for h in range(2):
+        activate(e, partial[e, 0], partial[e, 1])
+    for mine, theirs in ((sibling, tp), (tp, sibling)):
         for e in range(local):
-            down(last, e, h)
-        p_copy(last, h).start()
+            y = dot(hid[e, each:2 * each, :], wd[e, :, half(theirs)])
+            p_sib[last, theirs, e * each:(e + 1) * each, :] = y.astype(BF16)
+        p_copy(last, theirs).start()
+        for e in range(local):
+            y = dot(hid[e, 0:each, :], wd[e, :, half(mine)])
+            p_own[last, mine, e * each:(e + 1) * each, :] = y.astype(BF16)
 
     def rs_copy(src, k, at, part):
         span = pl.ds(part[0], part[1] - part[0])
@@ -354,11 +362,13 @@
         at = c + sibling * half_ch
         return jnp.where(at >= nch, at - nch, at)
 
-    for h in range(2):
+    for h in (sibling, tp):
         p_copy(last, h).wait_recv()
-        for c in range(h * half_ch, (h + 1) * half_ch):
-            combine(last, c)
-            rs0[c, 0:need(slots - 1), :] = contrib[slots - 1, c, 0:need(slots - 1), :].astype(BF16)
+        for at in range(half_ch):
+            combine(last, h, at)
+            c = h * half_ch + at
+            count = need(slots - 1)
+            rs0[c, 0:count, :] = contrib[slots - 1, c, 0:count, :].astype(BF16)
             skip_copy(c).start()
             k, count = slots - 2, need(slots - 2)
             rs[k, c, 0:count, :] = contrib[k, c, 0:count, :].astype(BF16)
@@ -506,6 +516,7 @@
             vmem((local, 2 * BATCH * cap, ffl), BF16),
             vmem((rows, BATCH * rows), BF16),
             vmem((nch, local * cap, CW), BF16),
+            vmem((2, 2 * BATCH * cap, ffl), F32),
             dma((slots,)), dma((slots + 2, width // LANES)), dma((slots + 1,)),
             dma((batches, 2)), dma((batches, 2)), dma((batches, 2)), dma((batches, 2)),
             dma((nch // 2,)), dma((nch // 2,)), dma((3,)), dma,

time: 125 us -> 123 us (0.984)
    pallas_call x1, Pallas kernels: 124 us -> 123 us  [on_device(): pl.pallas_call(functools.partial(kernel, n, rows, width, local, cap, grou...]
where the time goes in v5:
time: 123 us
  Pallas kernels  123 us (100%)
    pallas_call x1, Pallas kernels, on_device(): pl.pallas_call(functools.partial(kernel, n, rows, width, local, cap, grou...  123 us

profile of v5, /device:TPU:37, one launch (start us, length us, event | category | flops | bytes accessed | tf_op | source)
XLA Modules:
  0.0 123.3 jit_solution(14539857830081089819)
XLA Ops:
  0.0 122.7 %shard_map.82 = bf16[64,1024]{1,0:T(8,128)(2,1)S(1)} custom-call(bf16[64,2048]{1,0:T(8,128)(2,1)} %tok_ref.1, f32[1,2048]{1,0:T(1,128)} %bitcast.4, s32[1,64]{1,0:T(1,128)} %bitcast.7, s32[4,64]{1,0:T(4,128)} %bitcast.5, f32[4,64]{1,0:T(4,128)} %bitcast.6, bf16[2,2048,256]{2,1,0:T(8,128)(2,1)} %wg_hbm.1, bf16[2,2048,256]{2,1,0:T(8,128)(2,1)} %wu_hbm.1, ...), custom_call_target="tpu_custom_call" | custom-call | tf_op jit(solution)/shard_map/pallas_call | solution.py:491
  122.7 0.7 copy.10

commit v6 on v5

--- a/solution.py
+++ b/solution.py
@@ -191,7 +191,7 @@
             sel[e * each:(e + 1) * each, :] = pick.astype(BF16)
             for p in range(3):
                 at = (p * local + e) * each
-                gsel[at:at + each, :] = (pick * gates[e][p]).astype(BF16)
+                gsel[lax.rem(b, 2), at:at + each, :] = (pick * gates[e][p]).astype(BF16)
 
     def select(b, c):
         block = jnp.concatenate([
@@ -232,7 +232,7 @@
     def combine(b, h, at):
         cols = slice(at * CW, (at + 1) * CW)
         y = (p_own[b, h, :, cols].astype(F32) + p_rcv[b, h, :, cols].astype(F32)).astype(BF16)
-        g = tdot(gsel[...], jnp.concatenate([y, y, y], axis=0))
+        g = tdot(gsel[lax.rem(b, 2)], jnp.concatenate([y, y, y], axis=0))
         for j in range(BATCH):
             contrib[b * BATCH + j, h * half_ch + at] = g[j * rows:(j + 1) * rows]
 
@@ -243,13 +243,10 @@
             work[1 + c] = [call(select, b, c)]
         for h in range(2):
             work[(h + 1) * half_ch].append(lambda h=h: x_copy(b, h).start())
-            work[12 + h] = [lambda h=h: x_copy(b, h).wait_recv(), call(gate_up, b, 0, h)]
-            work[14 + h] = [call(down, b, 0, h)]
-            work[16 + h] = [call(gate_up, b, 1, h)]
-            work[18 + h] = [call(down, b, 1, h), lambda h=h: p_copy(b, h).start()]
-            for at in range(half_ch):
-                work[24 + h * half_ch + at] = [call(combine, b, h, at)]
-            work[24 + h * half_ch].insert(0, lambda h=h: p_copy(b, h).wait_recv())
+            work[17 + h] = [lambda h=h: x_copy(b, h).wait_recv(), call(gate_up, b, 0, h)]
+            work[19 + h] = [call(down, b, 0, h)]
+            work[21 + h] = [call(gate_up, b, 1, h)]
+            work[23 + h] = [call(down, b, 1, h), lambda h=h: p_copy(b, h).start()]
 
         def joined(calls):
             def go():
@@ -258,6 +255,16 @@
             return go
 
         return {at: joined(calls) for at, calls in work.items()}
+
+    def combine_at(b, i):
+        h, at = divmod(i, half_ch)
+        if at == 0:
+            p_copy(b, h).wait_recv()
+        combine(b, h, at)
+
+    def combine_place(b, i):
+        if 9 <= i < 9 + nch:
+            combine_at(b, i - 9)
 
     def ag_step(b, j, c, final):
         k = b * BATCH + j
@@ -291,6 +298,7 @@
                 ag_step(b, j, c, False)
             if i in work:
                 pl.when(b > 0)(work[i])
+            pl.when(b > 1)(functools.partial(combine_place, b - 2, i))
             if i == 10:
                 @pl.when(b == 1)
                 def _():
@@ -307,6 +315,7 @@
             ag_step(last, j, c, True)
         if i in work:
             work[i]()
+        combine_place(last - 2, i)
 
     for c in range(fine):
         ag_step(last, BATCH - 1, c, True)
@@ -317,6 +326,8 @@
             select(last, done - 1)
             if done in (half_ch, nch):
                 x_copy(last, done // half_ch - 1).start()
+    for i in range(half_ch):
+        combine_at(last - 1, i)
     partial = {}
     for h in range(2):
         x_copy(last, h).wait_recv()
@@ -335,6 +346,9 @@
         for e in range(local):
             y = dot(hid[e, 0:each, :], wd[e, :, half(mine)])
             p_own[last, mine, e * each:(e + 1) * each, :] = y.astype(BF16)
+
+    for i in range(half_ch, nch):
+        combine_at(last - 1, i)
 
     def rs_copy(src, k, at, part):
         span = pl.ds(part[0], part[1] - part[0])
@@ -509,7 +523,7 @@
             vmem((batches, 2, batch_rows, width // 2), BF16),
             vmem((nch // 2, rows, CW), BF16),
             vmem((batch_rows, BATCH * rows), BF16),
-            vmem((3 * batch_rows, BATCH * rows), BF16),
+            vmem((2, 3 * batch_rows, BATCH * rows), BF16),
             vmem((META, BATCH * rows), F32),
             vmem((8, BATCH * rows), F32),
             vmem((BATCH * rows, BATCH * rows), BF16),

time: 123 us -> 123 us (level)
  no operation moved by 1% of the time
where the time goes in v6:
time: 123 us
  Pallas kernels  122 us (99%)
    pallas_call x1, Pallas kernels, on_device(): pl.pallas_call(functools.partial(kernel, n, rows, width, local, cap, grou...  122 us

profile of v6, /device:TPU:37, one launch (start us, length us, event | category | flops | bytes accessed | tf_op | source)
XLA Modules:
  0.0 122.5 jit_solution(3936088594625984825)
XLA Ops:
  0.0 121.9 %shard_map.82 = bf16[64,1024]{1,0:T(8,128)(2,1)S(1)} custom-call(bf16[64,2048]{1,0:T(8,128)(2,1)} %tok_ref.1, f32[1,2048]{1,0:T(1,128)} %bitcast.4, s32[1,64]{1,0:T(1,128)} %bitcast.7, s32[4,64]{1,0:T(4,128)} %bitcast.5, f32[4,64]{1,0:T(4,128)} %bitcast.6, bf16[2,2048,256]{2,1,0:T(8,128)(2,1)} %wg_hbm.1, bf16[2,2048,256]{2,1,0:T(8,128)(2,1)} %wu_hbm.1, ...), custom_call_target="tpu_custom_call" | custom-call | tf_op jit(solution)/shard_map/pallas_call | solution.py:505
  121.9 0.7 copy.10

commit v7 on v6

--- a/solution.py
+++ b/solution.py
@@ -326,8 +326,6 @@
             select(last, done - 1)
             if done in (half_ch, nch):
                 x_copy(last, done // half_ch - 1).start()
-    for i in range(half_ch):
-        combine_at(last - 1, i)
     partial = {}
     for h in range(2):
         x_copy(last, h).wait_recv()
@@ -347,9 +345,6 @@
             y = dot(hid[e, 0:each, :], wd[e, :, half(mine)])
             p_own[last, mine, e * each:(e + 1) * each, :] = y.astype(BF16)
 
-    for i in range(half_ch, nch):
-        combine_at(last - 1, i)
-
     def rs_copy(src, k, at, part):
         span = pl.ds(part[0], part[1] - part[0])
         return pltpu.make_async_remote_copy(
@@ -388,6 +383,9 @@
             rs[k, c, 0:count, :] = contrib[k, c, 0:count, :].astype(BF16)
             for part in parts(count):
                 rs_copy(rs.at[k], k - 1, c, part).start()
+
+    for i in range(nch):
+        combine_at(last - 1, i)
 
     def rs_add(k, to, at, there, count, skipped=0):
         for lo, hi in parts(count):

time: 123 us -> 123 us (level)
  no operation moved by 1% of the time
where the time goes in v7:
time: 123 us
  Pallas kernels  122 us (99%)
    pallas_call x1, Pallas kernels, on_device(): pl.pallas_call(functools.partial(kernel, n, rows, width, local, cap, grou...  122 us

profile of v7, /device:TPU:37, one launch (start us, length us, event | category | flops | bytes accessed | tf_op | source)
XLA Modules:
  0.0 122.5 jit_solution(14548467439942917818)
XLA Ops:
  0.0 121.9 %shard_map.82 = bf16[64,1024]{1,0:T(8,128)(2,1)S(1)} custom-call(bf16[64,2048]{1,0:T(8,128)(2,1)} %tok_ref.1, f32[1,2048]{1,0:T(1,128)} %bitcast.4, s32[1,64]{1,0:T(1,128)} %bitcast.7, s32[4,64]{1,0:T(4,128)} %bitcast.5, f32[4,64]{1,0:T(4,128)} %bitcast.6, bf16[2,2048,256]{2,1,0:T(8,128)(2,1)} %wg_hbm.1, bf16[2,2048,256]{2,1,0:T(8,128)(2,1)} %wu_hbm.1, ...), custom_call_target="tpu_custom_call" | custom-call | tf_op jit(solution)/shard_map/pallas_call | solution.py:503
  121.9 0.7 copy.10
